TPU v7x, 32 devices: a whole 2x2x4 slice. The times are simulated.
32 devices in a mesh: ep: 8 (over z, core), tp: 4 (over y, x).
Axes of the slice: x: 2, y: 2, z: 4, core: 2. Of those that a mesh axis runs over, the one named last changes fastest.
Arguments:
- mix_rows: bfloat16 [2048, 2048], P('ep', 'tp'), may hold values from -6 to 6
- mix_gain: bfloat16 [2048], replicated, may hold values from 0.099609375 to 1.8984375
- w_query: bfloat16 [2048, 2048], P(None, 'tp'), may hold values from -0.125 to 0.125
- w_forget: bfloat16 [2048, 2048], P(None, 'tp'), may hold values from -0.125 to 0.125
- w_input: bfloat16 [2048, 2048], P(None, 'tp'), may hold values from -0.125 to 0.125
- w_outgate: bfloat16 [2048, 2048], P(None, 'tp'), may hold values from -0.125 to 0.125
- forget_gap: float32 [2048], P('tp'), may hold values from 1e-05 to 0.1
- decay_extra: float32 [16, 2048], P('tp', 'ep'), may hold values from -0.7 to 0, as said below
- head_gain: bfloat16 [128], replicated, may hold values from 0.099609375 to 1.8984375
- w_mixout: bfloat16 [2048, 2048], P('tp'), may hold values from -0.125 to 0.125
- moe_rows: bfloat16 [2048, 2048], P('ep', 'tp'), may hold values from -6 to 6
- moe_gain: bfloat16 [2048], replicated, may hold values from 0.099609375 to 1.8984375
- route_ids: int32 [2048, 2], P('ep'), may hold values from 0 to 7, all different within a row; in each aligned block of 256 rows (0 to 255, 256 to 511, ...) at most 96 rows name the same one
- route_scores: float32 [2048, 2], P('ep'), may hold values from 0.05 to 1
- w_gate: bfloat16 [8, 2048, 3072], P('ep', None, 'tp'), may hold values from -0.125 to 0.125
- w_up: bfloat16 [8, 2048, 3072], P('ep', None, 'tp'), may hold values from -0.125 to 0.125
- w_down: bfloat16 [8, 3072, 2048], P('ep', 'tp'), may hold values from -0.109375 to 0.109375
Outputs:
- mix_out: bfloat16 [2048, 2048], P('ep', 'tp')
- moe_out: bfloat16 [2048, 2048], P('ep', 'tp')
Inputs may be any that keep to these rules, and one draw needn't show every extreme that they name: `route_ids`: each row names 2 different experts. Among the rows of one index of ep at most 96 name the same expert, a bound that at least one block reaches. `decay_extra`: never positive.
All inputs are finite; a program needn't handle non-finite values.
Results may differ from a plain program's by a relative error of at most 0.017.
Values may be sent and summed in bfloat16 or wider, within the bound.
A program may use at most 64 MiB of HBM per device.

v0:
```python
import functools

import jax
import jax.numpy as jnp
from jax import lax
from jax.experimental import pallas as pl
from jax.experimental.pallas import tpu as pltpu
from jax.sharding import PartitionSpec as P

BLOCK = 64
epsilon = 1e-06
F32 = jnp.float32
BF16 = jnp.bfloat16
VMEM = pl.BlockSpec(memory_space=pltpu.VMEM)
LIMIT = 60 * 1024 * 1024


def dot(a, b, dims=((1,), (0,)), precision=None):
    return lax.dot_general(a, b, (dims, ((), ())), precision=precision, preferred_element_type=F32)


def sigmoid(x):
    return 1.0 / (1.0 + jnp.exp(-x))


def iota(shape, dim):
    return lax.broadcasted_iota(jnp.int32, shape, dim)


def mixer_kernel(per, x_ref, gain_ref, wq_ref, wf_ref, wi_ref, wo_ref, gap_ref, dec_ref,
                 lo_ref, qd_ref, og_ref, st_ref, normed):
    step = pl.program_id(0)
    length = normed.shape[0]
    dim = st_ref.shape[2]
    parts, _, cols = x_ref.shape

    @pl.when(step == 0)
    def _():
        total = jnp.zeros((length, 1), F32)
        for p in range(parts):
            v = x_ref[p].astype(F32)
            total += jnp.sum(v * v, axis=1, keepdims=True)
        scale = lax.rsqrt(total / (parts * cols) + epsilon)
        for p in range(parts):
            g = gain_ref[:, p * cols:(p + 1) * cols].astype(F32)
            normed[:, p * cols:(p + 1) * cols] = (x_ref[p].astype(F32) * scale * g).astype(BF16)

    n = normed[...]
    qp = dot(n, wq_ref[...])
    fp = dot(n, wf_ref[...])
    value = dot(n, wi_ref[...]).astype(BF16)
    op = dot(n, wo_ref[...])
    query = qp * sigmoid(qp)
    key = gap_ref[...] * sigmoid(-fp)
    og_ref[...] = op * sigmoid(op)
    logs = jnp.log1p(-key)
    dec = dec_ref[...]
    tri = (iota((length, length), 0) >= iota((length, length), 1)).astype(F32)
    causal = iota((BLOCK, BLOCK), 0) >= iota((BLOCK, BLOCK), 1)
    half = BLOCK // 2
    for j in range(per):
        c = slice(j * dim, (j + 1) * dim)
        extra = jnp.sum(jnp.where(iota(dec.shape, 1) == step * per + j, dec, 0.0), axis=1, keepdims=True)
        run = dot(tri, logs[:, c] + extra, precision=lax.Precision.HIGHEST)
        q, k, v = query[:, c], key[:, c], value[:, c]
        qd_ref[:, c] = (q * jnp.exp(run)).astype(BF16)
        state = jnp.zeros((dim, dim), F32)
        base = jnp.zeros((1, dim), F32)
        for b in range(length // BLOCK):
            r = slice(b * BLOCK, (b + 1) * BLOCK)
            g, qb, kb, vb = run[r], q[r], k[r], v[r]
            ref = g[half - 1:half]
            last = g[BLOCK - 1:BLOCK]
            qe = (qb * jnp.exp(g - ref)).astype(BF16)
            ke = (kb * jnp.exp(ref - g)).astype(BF16)
            scores = jnp.where(causal, dot(qe, ke, ((1,), (1,))), 0.0).astype(BF16)
            out = dot(scores, vb)
            if b:
                qs = (qb * jnp.exp(g - base)).astype(BF16)
                out += dot(qs, state.astype(BF16), ((1,), (1,)))
            lo_ref[r, c] = out
            kd = (kb * jnp.exp(last - g)).astype(BF16)
            state = state * jnp.exp(last - base) + dot(vb, kd, ((0,), (0,)))
            base = last
        st_ref[j, 0:dim, :] = state.astype(BF16)
        st_ref[j, dim:, :] = jnp.broadcast_to(jnp.exp(base), (st_ref.shape[1] - dim, dim)).astype(BF16)


def mixer(x, gain, wq, wf, wi, wo, gap, dec):
    parts, length, cols = x.shape
    heads, dim = dec.shape[1], wq.shape[1] // dec.shape[1]
    per = 2 if heads % 2 == 0 else 1
    width = per * dim
    depth = wq.shape[0]
    column = pl.BlockSpec((depth, width), lambda i: (0, i))
    rows = pl.BlockSpec((length, width), lambda i: (0, i))
    whole = lambda s: pl.BlockSpec(s, lambda i: (0,) * len(s))
    return pl.pallas_call(
        functools.partial(mixer_kernel, per),
        grid=(heads // per,),
        in_specs=[whole(x.shape), whole((1, depth)), column, column, column, column,
                  pl.BlockSpec((1, width), lambda i: (0, i)), whole(dec.shape)],
        out_specs=[rows, rows, rows, pl.BlockSpec((per, dim + 16, dim), lambda i: (i, 0, 0))],
        out_shape=[jax.ShapeDtypeStruct((length, heads * dim), F32),
                   jax.ShapeDtypeStruct((length, heads * dim), BF16),
                   jax.ShapeDtypeStruct((length, heads * dim), F32),
                   jax.ShapeDtypeStruct((heads, dim + 16, dim), BF16)],
        scratch_shapes=[pltpu.VMEM((length, depth), BF16)],
        compiler_params=pltpu.CompilerParams(vmem_limit_bytes=LIMIT),
        cost_estimate=pl.CostEstimate(flops=10 * 10**9, bytes_accessed=9 * 10**6, transcendentals=10**6),
    )(x, gain.reshape(1, -1), wq, wf, wi, wo, gap.reshape(1, -1), dec)


def tail_kernel(states_ref, lo_ref, qd_ref, og_ref, hg_ref, w_ref, out_ref, gated):
    place = lax.axis_index("ep")
    hops, heads, _, dim = states_ref.shape
    for h in range(heads):
        c = slice(h * dim, (h + 1) * dim)

        def one(hop, state):
            own = states_ref[hop, h, 0:dim, :].astype(F32)
            passing = states_ref[hop, h, dim:dim + 16, :].astype(F32)[0:1]
            return jnp.where(hop < place, state * passing + own, state)

        state = lax.fori_loop(0, hops, one, jnp.zeros((dim, dim), F32))
        out = lo_ref[:, c] + dot(qd_ref[:, c], state.astype(BF16), ((1,), (1,)))
        scale = lax.rsqrt(jnp.mean(out * out, axis=1, keepdims=True) + epsilon)
        gated[:, c] = (out * scale * hg_ref[...].astype(F32) * og_ref[:, c]).astype(BF16)
    parts, _, cols = out_ref.shape
    for p in range(parts):
        out_ref[p] = dot(gated[...], w_ref[:, p * cols:(p + 1) * cols]).astype(BF16)


def tail(states, lo, qd, og, hg, w, parts):
    length, width = lo.shape
    return pl.pallas_call(
        tail_kernel,
        in_specs=[VMEM] * 6,
        out_specs=VMEM,
        out_shape=jax.ShapeDtypeStruct((parts, length, w.shape[1] // parts), BF16),
        scratch_shapes=[pltpu.VMEM((length, width), BF16)],
        compiler_params=pltpu.CompilerParams(vmem_limit_bytes=LIMIT),
        cost_estimate=pl.CostEstimate(flops=10**9, bytes_accessed=5 * 10**6, transcendentals=10**5),
    )(states, lo, qd, og, hg.reshape(1, -1), w)


def ranks(ids, experts):
    tokens = ids.shape[1]
    names = iota((experts, tokens), 0)
    picks = [names == ids[k:k + 1, :] for k in range(ids.shape[0])]
    chosen = functools.reduce(jnp.logical_or, picks)
    before = (iota((tokens, tokens), 0) < iota((tokens, tokens), 1)).astype(BF16)
    return picks, chosen, dot(chosen.astype(BF16), before)


def slot_hits(mask, rank, experts, capacity):
    rows = experts * capacity
    owner = iota((rows, experts), 0) - iota((rows, experts), 1) * capacity
    owner = jnp.logical_and(owner >= 0, owner < capacity).astype(F32)
    tokens = rank.shape[1]
    spread = dot(owner, jnp.where(mask, rank, -1.0))
    spot = dot(owner, iota((experts, tokens), 0).astype(F32)) * capacity
    return (spread >= 0.0) & (spread + spot == iota((rows, tokens), 0).astype(F32))


def dispatch_kernel(experts, capacity, ids_ref, rows_ref, out_ref):
    _, chosen, rank = ranks(ids_ref[...], experts)
    hits = slot_hits(chosen, rank, experts, capacity).astype(BF16)
    out_ref[...] = dot(hits, rows_ref[...]).astype(BF16)


def dispatch(ids, rows, experts, capacity):
    return pl.pallas_call(
        functools.partial(dispatch_kernel, experts, capacity),
        in_specs=[VMEM] * 2,
        out_specs=VMEM,
        out_shape=jax.ShapeDtypeStruct((experts * capacity, rows.shape[1]), BF16),
    )(ids, rows)


def combine_kernel(experts, capacity, ids_ref, scores_ref, back_ref, out_ref):
    picks, _, rank = ranks(ids_ref[...], experts)
    scores = scores_ref[...]
    weights = scores / jnp.sum(scores, axis=1, keepdims=True)
    total = jnp.zeros(out_ref.shape, F32)
    for k, mask in enumerate(picks):
        hits = slot_hits(mask, rank, experts, capacity).astype(BF16)
        total += dot(hits, back_ref[...], ((0,), (0,))) * weights[:, k:k + 1]
    out_ref[...] = total.astype(BF16)


def combine(ids, scores, back, experts, capacity):
    return pl.pallas_call(
        functools.partial(combine_kernel, experts, capacity),
        in_specs=[VMEM] * 3,
        out_specs=VMEM,
        out_shape=jax.ShapeDtypeStruct((ids.shape[1], back.shape[1]), BF16),
    )(ids, scores, back)


def expert_kernel(x_ref, gain_ref, wg_ref, wu_ref, wd_ref, out_ref, normed, total):
    step = pl.program_id(0)
    parts, rows, cols = x_ref.shape

    @pl.when(step == 0)
    def _():
        squares = jnp.zeros((rows, 1), F32)
        for p in range(parts):
            v = x_ref[p].astype(F32)
            squares += jnp.sum(v * v, axis=1, keepdims=True)
        scale = lax.rsqrt(squares / (parts * cols) + epsilon)
        for p in range(parts):
            g = gain_ref[:, p * cols:(p + 1) * cols].astype(F32)
            normed[:, p * cols:(p + 1) * cols] = (x_ref[p].astype(F32) * scale * g).astype(BF16)

    gate = dot(normed[...], wg_ref[0])
    up = dot(normed[...], wu_ref[0])
    hidden = (gate * sigmoid(gate) * up).astype(BF16)
    last = pl.num_programs(0) - 1
    for p in range(parts):
        c = slice(p * cols, (p + 1) * cols)
        part = dot(hidden, wd_ref[0, :, c])

        @pl.when(jnp.logical_and(step == 0, last > 0))
        def _():
            total[:, c] = part

        @pl.when(jnp.logical_and(step > 0, step < last))
        def _():
            total[:, c] += part

        @pl.when(step == last)
        def _():
            out_ref[p] = (jnp.where(step > 0, total[:, c], 0.0) + part).astype(BF16)


def experts_call(x, gain, wg, wu, wd):
    parts, rows, cols = x.shape
    depth, units = wg.shape[1:]
    tile = 256 if units % 256 == 0 else units
    return pl.pallas_call(
        expert_kernel,
        grid=(units // tile,),
        in_specs=[pl.BlockSpec(x.shape, lambda i: (0, 0, 0)), pl.BlockSpec((1, depth), lambda i: (0, 0)),
                  pl.BlockSpec((1, depth, tile), lambda i: (0, 0, i)),
                  pl.BlockSpec((1, depth, tile), lambda i: (0, 0, i)),
                  pl.BlockSpec((1, tile, depth), lambda i: (0, i, 0))],
        out_specs=pl.BlockSpec(x.shape, lambda i: (0, 0, 0)),
        out_shape=jax.ShapeDtypeStruct(x.shape, BF16),
        scratch_shapes=[pltpu.VMEM((rows, depth), BF16), pltpu.VMEM((rows, depth), F32)],
        compiler_params=pltpu.CompilerParams(vmem_limit_bytes=LIMIT),
        cost_estimate=pl.CostEstimate(flops=8 * 10**9, bytes_accessed=10**7, transcendentals=10**6),
    )(x, gain.reshape(1, -1), wg, wu, wd)


def per_device(mix_rows, mix_gain, w_query, w_forget, w_input, w_outgate, forget_gap, decay_extra,
               head_gain, w_mixout, moe_rows, moe_gain, route_ids, route_scores, w_gate, w_up, w_down):
    eps, tps = lax.axis_size("ep"), lax.axis_size("tp")
    tokens, top = route_ids.shape
    experts = w_gate.shape[0] * eps
    capacity = tokens * top * 3 // (2 * experts)
    cols = mix_rows.shape[1]
    ids = route_ids.T
    slots = dispatch(ids, moe_rows, experts, capacity)
    arrived = lax.all_to_all(slots.reshape(eps, -1, cols), "ep", split_axis=0, concat_axis=0, tiled=True)
    gathered = lax.all_gather(arrived.reshape(-1, cols), "tp", axis=0)
    mix_whole = lax.all_gather(mix_rows, "tp", axis=0)
    lo, qd, og, st = mixer(mix_whole, mix_gain, w_query, w_forget, w_input, w_outgate, forget_gap, decay_extra.T)
    product = experts_call(gathered, moe_gain, w_gate, w_up, w_down)
    expert_sum = lax.psum_scatter(product, "tp", scatter_dimension=0)
    states = lax.all_gather(st, "ep", axis=0)
    mixed = tail(states, lo, qd, og, head_gain, w_mixout, tps)
    mix_out = lax.psum_scatter(mixed, "tp", scatter_dimension=0)
    back = lax.all_to_all(expert_sum.reshape(eps, -1, cols), "ep", split_axis=0, concat_axis=0, tiled=True)
    moe_out = combine(ids, route_scores, back.reshape(-1, cols), experts, capacity)
    return (mix_out, moe_out)


def solution(mesh):
    placed = (
        P("ep", "tp"), P(), P(None, "tp"), P(None, "tp"), P(None, "tp"), P(None, "tp"), P("tp"),
        P("tp", "ep"), P(), P("tp", None), P("ep", "tp"), P(), P("ep", None), P("ep", None),
        P("ep", None, "tp"), P("ep", None, "tp"), P("ep", "tp", None),
    )
    return jax.shard_map(
        per_device, mesh=mesh, in_specs=placed,
        out_specs=(P("ep", "tp"), P("ep", "tp")), check_vma=False,
    )
```

profile of v0, /device:TPU:0, one launch (start us, length us, event | category | flops | bytes accessed | tf_op | source)
XLA Modules:
  0.0 194.2 jit_solution(4513498699415049200)
XLA Ops:
  7.2 0.0 copy-start.1
  7.2 0.0 copy-start.2
  7.2 0.0 all-gather.8.cloned.1.call-start
  7.2 0.7 all-gather.8.cloned.1.call-update
  7.9 0.0 all-gather.6.cloned.1.call-start
  8.0 2.6 %shard_map.178 = bf16[768,512]{1,0:T(8,128)(2,1)} custom-call(s32[2,256]{1,0:T(2,128)} %bitcast.18, bf16[256,512]{1,0:T(8,128)(2,1)} %rows_ref.1), custom_call_target="tpu_custom_call" | custom-call | tf_op jit(solution)/shard_map/pallas_call | solution.py:173
  10.5 27.4 %all_to_all.10 = bf16[8,96,512]{2,1,0:T(8,128)(2,1)} all-to-all(bf16[8,96,512]{2,1,0:T(8,128)(2,1)} %bitcast.14), channel_id=1, replica_groups=mesh['ep'=8,'tp'=4] {'ep'}, dimensions={0} | all-to-all | bytes 1572864 | tf_op jit(solution)/shard_map/all_to_all | solution.py:265
  37.9 0.0 all-gather.6.cloned.1.call-update
  38.0 0.0 all-gather.10.cloned.1.call-start
  38.0 0.0 copy-done.1
  38.0 0.8 copy.21
  38.8 0.0 copy-done.2
  38.8 0.6 reshape.22.gain_ref
  39.4 0.0 all-gather.8.cloned.1.call-done
  39.4 0.0 copy-start.3
  39.4 11.6 %shard_map.176 = (f32[256,512]{1,0:T(8,128)}, bf16[256,512]{1,0:T(8,128)(2,1)}, f32[256,512]{1,0:T(8,128)}, bf16[4,144,128]{2,1,0:T(8,128)(2,1)}) custom-call(bf16[4,256,512]{2,1,0:T(8,128)(2,1)} %bitcast.21, bf16[1,2048]{1,0:T(2,128)(2,1)} %reshape.22.gain_ref, bf16[2048,512]{1,0:T(8,128)(2,1)} %wq_ref.1, bf16[2048,512]{1,0:T(8,128)(2,1)} %wf_ref.1, ...), custom_call_target="tpu_custom_call" | custom-call | flops 10000000000 | bytes 9000000 | tf_op jit(solution)/shard_map/pallas_call | solution.py:98
  51.0 0.0 all-gather.10.cloned.1.call-update
  51.1 0.0 reduce-scatter.9.cloned.1.call-start
  51.1 0.0 copy-done.3
  51.1 0.6 reshape.26.gain_ref
  51.7 33.2 %all-gather.6.cloned.1.call-done.x_ref = bf16[4,768,512]{2,1,0:T(8,128)(2,1)} async-done(((bf16[1,768,512]{2,1,0:T(8,128)(2,1)}), bf16[4,768,512]{2,1,0:T(8,128)(2,1)}) %all-gather.6.cloned.1.call-update) | async-done | bytes 3145744 | tf_op jit(solution)/shard_map/all_gather | solution.py:266
  84.9 17.0 %shard_map.179 = bf16[4,768,512]{2,1,0:T(8,128)(2,1)} custom-call(bf16[4,768,512]{2,1,0:T(8,128)(2,1)} %all-gather.6.cloned.1.call-done.x_ref, bf16[1,2048]{1,0:T(2,128)(2,1)} %reshape.26.gain_ref, bf16[1,2048,768]{2,1,0:T(8,128)(2,1)} %wg_ref.1, bf16[1,2048,768]{2,1,0:T(8,128)(2,1)} %wu_ref.1, bf16[1,768,2048]{2,1,0:T(8,128)(2,1)} %wd_ref.1), custom_call_target="tpu_custom_call" | custom-call | flops 8000000000 | bytes 10000000 | tf_op jit(solution)/shard_map/pallas_call | solution.py:241
  102.0 0.0 reduce-scatter.9.cloned.1.call-update
  102.0 0.0 reduce-scatter.7.cloned.1.call-start
  102.1 7.9 %all-gather.10.cloned.1.call-done = bf16[32,144,128]{2,1,0:T(8,128)(2,1)} async-done(((bf16[4,144,128]{2,1,0:T(8,128)(2,1)}), bf16[32,144,128]{2,1,0:T(8,128)(2,1)}) %all-gather.10.cloned.1.call-update) | async-done | bytes 1179664 | tf_op jit(solution)/shard_map/all_gather | solution.py:271
  110.0 5.4 %shard_map.177 = bf16[4,256,512]{2,1,0:T(8,128)(2,1)} custom-call(bf16[8,4,144,128]{3,2,1,0:T(8,128)(2,1)} %bitcast.15, f32[256,512]{1,0:T(8,128)} %get-tuple-element.7.lo_ref, bf16[256,512]{1,0:T(8,128)(2,1)} %get-tuple-element.8.qd_ref, f32[256,512]{1,0:T(8,128)} %get-tuple-element.9.og_ref, bf16[1,128]{1,0:T(2,128)(2,1)} %bitcast.20, bf16[512,2048]{1,0:T(8,128)(2,1)} %w_ref.1), custom_call_target="tpu_custom_call" | custom-call | flops 1000000000 | bytes 5000000 | tf_op jit(solution)/shard_map/pallas_call | solution.py:136
  115.4 0.0 copy-start.4
  115.4 0.0 reduce-scatter.7.cloned.1.call-update
  115.4 40.9 %reduce-scatter.9.cloned.1.call-done = bf16[1,768,512]{2,1,0:T(8,128)(2,1)} async-done(((bf16[4,768,512]{2,1,0:T(8,128)(2,1)}), bf16[1,768,512]{2,1,0:T(8,128)(2,1)}) %reduce-scatter.9.cloned.1.call-update) | async-done | bytes 786448
  156.4 4.6 %all-to-all-start.1 = ((bf16[8,96,512]{2,1,0:T(8,128)(2,1)}), bf16[8,96,512]{2,1,0:T(8,128)(2,1)S(1)}, u32[]{:S(2)}, u32[]{:S(2)}) async-start(bf16[8,96,512]{2,1,0:T(8,128)(2,1)} %bitcast.16), calls=%async_computation.1 | async-start | bytes 1572864 | tf_op jit(solution)/shard_map/all_to_all | solution.py:274
  161.0 0.0 copy-done.4
  161.0 0.8 copy.22.scores_ref
  161.8 20.1 %all-to-all-done.1 = bf16[8,96,512]{2,1,0:T(8,128)(2,1)S(1)} async-done(((bf16[8,96,512]{2,1,0:T(8,128)(2,1)}), bf16[8,96,512]{2,1,0:T(8,128)(2,1)S(1)}, u32[]{:S(2)}, u32[]{:S(2)}) %all-to-all-start.1) | async-done | bytes 786464 | tf_op jit(solution)/shard_map/all_to_all | solution.py:274
  181.9 0.0 copy-start
  181.9 0.9 copy-done
  182.9 3.3 %shard_map.180 = bf16[256,512]{1,0:T(8,128)(2,1)} custom-call(s32[2,256]{1,0:T(2,128)} %bitcast.19, f32[256,2]{1,0:T(8,128)} %copy.22.scores_ref, bf16[768,512]{1,0:T(8,128)(2,1)} %bitcast.13), custom_call_target="tpu_custom_call" | custom-call | tf_op jit(solution)/shard_map/pallas_call | solution.py:193
  186.2 1.5 reduce-scatter.7.cloned.1.call-done
Async XLA Ops:
  7.2 30.8 %copy-start.1 = (f32[4,256]{1,0:T(4,128)S(1)}, f32[4,256]{1,0:T(4,128)}, u32[]{:S(2)}) copy-start(f32[4,256]{1,0:T(4,128)} %param.24) | copy-start | bytes 12292
  7.2 31.6 %copy-start.2 = (bf16[2048]{0:T(1024)(128)(2,1)S(1)}, bf16[2048]{0:T(1024)(128)(2,1)}, u32[]{:S(2)}) copy-start(bf16[2048]{0:T(1024)(128)(2,1)} %param.18) | copy-start | bytes 12292
  7.2 32.2 %all-gather.8.cloned.1.call-start = ((), (), s32[]{:S(2)}) async-start(), calls=%async_computation.5 | async-start | bytes 1310720 | tf_op jit(solution)/shard_map/all_gather | solution.py:267
  7.9 77.0 %all-gather.6.cloned.1.call-start = ((), (), s32[]{:S(2)}) async-start(), calls=%async_computation.4 | async-start | bytes 3932160 | tf_op jit(solution)/shard_map/all_gather | solution.py:266
  38.0 72.0 %all-gather.10.cloned.1.call-start = ((), (), s32[]{:S(2)}) async-start(), calls=%async_computation.6 | async-start | bytes 1327104 | tf_op jit(solution)/shard_map/all_gather | solution.py:271
  39.4 11.7 %copy-start.3 = (bf16[2048]{0:T(1024)(128)(2,1)S(1)}, bf16[2048]{0:T(1024)(128)(2,1)}, u32[]{:S(2)}) copy-start(bf16[2048]{0:T(1024)(128)(2,1)} %param.28) | copy-start | bytes 12292
  51.1 105.3 %reduce-scatter.9.cloned.1.call-start = ((), (), s32[]{:S(2)}) async-start(), calls=%async_computation.8 | async-start | bytes 3932160
  102.0 85.7 %reduce-scatter.7.cloned.1.call-start = ((), (), s32[]{:S(2)}) async-start(), calls=%async_computation.7 | async-start | bytes 1310720
  115.4 45.6 %copy-start.4 = (f32[256,2]{0,1:T(2,128)S(1)}, f32[256,2]{0,1:T(2,128)}, u32[]{:S(2)}) copy-start(f32[256,2]{0,1:T(2,128)} %param.30) | copy-start | bytes 6148
  156.4 25.6 %all-to-all-start.1 = ((bf16[8,96,512]{2,1,0:T(8,128)(2,1)}), bf16[8,96,512]{2,1,0:T(8,128)(2,1)S(1)}, u32[]{:S(2)}, u32[]{:S(2)}) async-start(bf16[8,96,512]{2,1,0:T(8,128)(2,1)} %bitcast.16), calls=%async_computation.1 | async-start | bytes 1572864 | tf_op jit(solution)/shard_map/all_to_all | solution.py:274
  181.9 0.9 copy-start
Sparse Core Ops, SparseCore 0:
  9.8 29.2 all-gather.7
  40.9 43.9 all-gather.5
  87.2 22.7 all-gather.9
  112.8 43.5 reduce-scatter.8
  159.7 27.9 reduce-scatter.6
where the time goes:
time: 195 us; the launch traced here: 194 us
  waiting for transfers between devices  104 us (53%)
  Pallas kernels  40 us (21%)
  blocking collectives  27.4 us (14%)
  between operations  13.8 us (7%)
  starting transfers between devices  4.81 us (2%)
  local copies, waits for them, and re-layouts  3.74 us (2%)
    unnamed x7, waiting for transfers between devices  43.2 us
    all_gather x1, waiting for transfers between devices, per_device(): gathered = lax.all_gather(arrived.reshape(-1, cols), 'tp', axis=0)  33.2 us
    all_to_all x1, blocking collectives, per_device(): lax.all_to_all(slots.reshape(eps, -1, cols), 'ep', split_axis=0, concat_a...  27.4 us
    all_to_all x1, waiting for transfers between devices, per_device(): lax.all_to_all(expert_sum.reshape(eps, -1, cols), 'ep', split_axis=0, con...  20.1 us
    pallas_call x1, Pallas kernels, experts_call(): pl.pallas_call(expert_kernel, grid=(units // tile,), in_specs=[pl.BlockSp...  17 us
    pallas_call x1, Pallas kernels, mixer(): pl.pallas_call(functools.partial(mixer_kernel, per), grid=(heads // per,)...  11.6 us
    all_gather x1, waiting for transfers between devices, per_device(): states = lax.all_gather(st, 'ep', axis=0)  7.91 us
    pallas_call x1, Pallas kernels, tail(): pl.pallas_call(tail_kernel, in_specs=[VMEM] * 6, out_specs=VMEM, out_shap...  5.45 us
  transfers between devices with their start and end apart: 6, of which 5 were waited for; matrix products, arithmetic and copies ran while one was open for 1% of the time, Pallas kernels for 21%

commit v1 on v0

--- a/solution.py
+++ b/solution.py
@@ -252,10 +252,374 @@
         cost_estimate=pl.CostEstimate(flops=8 * 10**9, bytes_accessed=10**7, transcendentals=10**6),
     )(x, gain.reshape(1, -1), wg, wu, wd)
 
+MESH = pl.DeviceIdType.MESH
+ANY = pl.BlockSpec(memory_space=pl.ANY)
+HIGHEST = lax.Precision.HIGHEST
+GROUPS = 2
+
+
+def flip(place, bits):
+    bit = 1
+    while bit <= bits:
+        if bits & bit:
+            place = place + bit - 2 * bit * lax.rem(lax.div(place, bit), 2)
+        bit *= 2
+    return place
+
+
+def block_kernel(cap, mix_ref, mgain_ref, wq_hbm, wf_hbm, wi_hbm, wo_hbm, gap_ref, dec_ref, hgain_ref, wm_hbm,
+                 moe_ref, egain_ref, ids_ref, scores_ref, wg_hbm, wu_hbm, wd_hbm,
+                 mix_out, moe_out,
+                 wmix, wm, wg, wu, wd, xall, normed, lo, qd, og, st, states, gated, mixed, mixin,
+                 gath, slots, hits, enormed, hidden, psend, precv, esum, back, total,
+                 wsem, xs, xr, zs, zr, gs, gr, ps, pr, bs, br, ss, sr, ms, mr):
+    eps, tps = lax.axis_size("ep"), lax.axis_size("tp")
+    me, mt = lax.axis_index("ep"), lax.axis_index("tp")
+    length, cols = mix_ref.shape
+    rows = eps * cap
+    heads, _, dim = st.shape
+    depth = tps * cols
+    units = wg.shape[1]
+    ep_peer = [flip(me, k) for k in range(eps)]
+    tp_peer = [flip(mt, r) for r in range(tps)]
+
+    def push(src, dst, send, recv, ep=None, tp=None):
+        where = {"ep": ep_peer[ep]} if tp is None else {"tp": tp_peer[tp]}
+        return pltpu.make_async_remote_copy(src_ref=src, dst_ref=dst, send_sem=send, recv_sem=recv,
+                                            device_id=where, device_id_type=MESH)
+
+    sent = []
+
+    def go(copy):
+        copy.start()
+        sent.append(copy)
+
+    loads = [pltpu.make_async_copy(s, wmix.at[i], wsem.at[i]) for i, s in enumerate((wq_hbm, wf_hbm, wi_hbm, wo_hbm))]
+    loads += [pltpu.make_async_copy(wg_hbm.at[0], wg, wsem.at[4]), pltpu.make_async_copy(wu_hbm.at[0], wu, wsem.at[5]),
+              pltpu.make_async_copy(wd_hbm.at[0], wd, wsem.at[6]), pltpu.make_async_copy(wm_hbm, wm, wsem.at[7])]
+    for load in loads:
+        load.start()
+
+    barrier = pltpu.get_barrier_semaphore()
+    for k in range(1, eps):
+        pl.semaphore_signal(barrier, inc=1, device_id={"ep": ep_peer[k]}, device_id_type=MESH)
+    for r in range(1, tps):
+        pl.semaphore_signal(barrier, inc=1, device_id={"tp": tp_peer[r]}, device_id_type=MESH)
+    pl.semaphore_wait(barrier, eps + tps - 2)
+
+    half = length // 2
+    go(push(mix_ref, xall.at[mt], xs.at[0], xr.at[0], tp=1))
+    go(push(mix_ref, xall.at[mt], xs.at[1], xr.at[1], tp=2))
+
+    experts = eps
+    names = iota((length, experts), 1)
+    ids = ids_ref[...]
+    picks = [ids[:, j:j + 1] == names for j in range(ids.shape[1])]
+    chosen = functools.reduce(jnp.logical_or, picks)
+    before = (iota((length, length), 0) > iota((length, length), 1)).astype(BF16)
+    rank = dot(before, chosen.astype(BF16)).astype(jnp.int32)
+    spot = rank + jnp.bitwise_xor(names, me) * cap
+    both = None
+    for j, pick in enumerate(picks):
+        at = jnp.sum(jnp.where(pick, spot, 0), axis=1, keepdims=True)
+        hit = (iota((length, rows), 1) == at).astype(F32)
+        hits[j] = hit.astype(BF16)
+        both = hit if both is None else both + hit
+    made = dot(both.astype(BF16), moe_ref[...], ((0,), (0,))).astype(BF16)
+    slots[...] = made
+    gath[mt, 0:cap, :] = made[0:cap]
+    for k in range(1, eps):
+        r = slice(k * cap, (k + 1) * cap)
+        go(push(slots.at[r], gath.at[mt, r], zs.at[k], zr.at[k], ep=k))
+
+    def rowsof(k, part=None):
+        if part is None:
+            return pl.ds(k * cap, cap)
+        return pl.ds(k * cap + part * (cap // 2), cap // 2)
+
+    def spread(k):
+        if k:
+            push(slots.at[rowsof(k)], gath.at[mt, rowsof(k)], zs.at[k], zr.at[k], ep=k).wait_recv()
+        for n, r in enumerate((1, 2)):
+            ref = gath.at[mt, rowsof(k)]
+            go(push(ref, ref, gs.at[k, n], gr.at[k, n], tp=r))
+
+    def relay(k):
+        for n, (source, target) in enumerate(((1, 2), (2, 1))):
+            whole = gath.at[tp_peer[source], rowsof(k)]
+            push(whole, whole, gs.at[k, n], gr.at[k, n], tp=source).wait_recv()
+            ref = gath.at[tp_peer[source], rowsof(k, n)]
+            go(push(ref, ref, gs.at[k, 2 + n], gr.at[k, 2 + n], tp=target))
+
+    def complete(k):
+        for n, via in enumerate((2, 1)):
+            ref = gath.at[tp_peer[3], rowsof(k, n)]
+            push(ref, ref, gs.at[k, 2 + n], gr.at[k, 2 + n], tp=via).wait_recv()
+
+    def relay_mix():
+        for n, (source, target) in enumerate(((1, 2), (2, 1))):
+            whole = xall.at[tp_peer[source]]
+            push(whole, whole, xs.at[n], xr.at[n], tp=source).wait_recv()
+            ref = xall.at[tp_peer[source], pl.ds(n * half, half)]
+            go(push(ref, ref, xs.at[2 + n], xr.at[2 + n], tp=target))
+
+    def complete_mix():
+        for n, via in enumerate((2, 1)):
+            ref = xall.at[tp_peer[3], pl.ds(n * half, half)]
+            push(ref, ref, xs.at[2 + n], xr.at[2 + n], tp=via).wait_recv()
+
+    agenda = [functools.partial(spread, 0), relay_mix, functools.partial(spread, 1), functools.partial(relay, 0)]
+    for k in range(2, eps):
+        agenda += [functools.partial(spread, k), functools.partial(relay, k - 1)]
+    agenda.append(functools.partial(relay, eps - 1))
+
+    def poll(count=1):
+        for _ in range(min(count, len(agenda))):
+            agenda.pop(0)()
+
+    poll(4)
+    xall[mt] = mix_ref[...]
+    complete_mix()
+    squares = jnp.zeros((length, 1), F32)
+    for p in range(tps):
+        v = xall[p].astype(F32)
+        squares += jnp.sum(v * v, axis=1, keepdims=True)
+    scale = lax.rsqrt(squares / depth + epsilon)
+    for p in range(tps):
+        c = slice(p * cols, (p + 1) * cols)
+        normed[:, c] = (xall[p].astype(F32) * scale * mgain_ref[:, c].astype(F32)).astype(BF16)
+    poll(1)
+
+    tri = (iota((length, length), 0) >= iota((length, length), 1)).astype(F32)
+    extra = dot(tri, dec_ref[...], ((1,), (1,)), precision=HIGHEST)
+    causal = iota((BLOCK, BLOCK), 0) >= iota((BLOCK, BLOCK), 1)
+    mid = BLOCK // 2
+    per = 2 if heads % 2 == 0 else 1
+    for load in loads[:4]:
+        load.wait()
+    for step in range(heads // per):
+        w = slice(step * per * dim, (step + 1) * per * dim)
+        n = normed[...]
+        qp = dot(n, wmix[0, :, w])
+        fp = dot(n, wmix[1, :, w])
+        value = dot(n, wmix[2, :, w]).astype(BF16)
+        op = dot(n, wmix[3, :, w])
+        query = qp * sigmoid(qp)
+        key = gap_ref[:, w] * sigmoid(-fp)
+        og[:, w] = op * sigmoid(op)
+        logs = jnp.log1p(-key)
+        poll(1)
+        for j in range(per):
+            h = step * per + j
+            cl = slice(j * dim, (j + 1) * dim)
+            c = slice(h * dim, (h + 1) * dim)
+            run = dot(tri, logs[:, cl], precision=HIGHEST) + extra[:, h:h + 1]
+            q, k, v = query[:, cl], key[:, cl], value[:, cl]
+            qd[:, c] = (q * jnp.exp(run)).astype(BF16)
+            state = jnp.zeros((dim, dim), F32)
+            base = jnp.zeros((1, dim), F32)
+            for b in range(length // BLOCK):
+                r = slice(b * BLOCK, (b + 1) * BLOCK)
+                g, qb, kb, vb = run[r], q[r], k[r], v[r]
+                ref = g[mid - 1:mid]
+                last = g[BLOCK - 1:BLOCK]
+                qe = (qb * jnp.exp(g - ref)).astype(BF16)
+                ke = (kb * jnp.exp(ref - g)).astype(BF16)
+                scores = jnp.where(causal, dot(qe, ke, ((1,), (1,))), 0.0).astype(BF16)
+                out = dot(scores, vb)
+                if b:
+                    qs = (qb * jnp.exp(g - base)).astype(BF16)
+                    out += dot(qs, state.astype(BF16), ((1,), (1,)))
+                lo[r, c] = out
+                kd = (kb * jnp.exp(last - g)).astype(BF16)
+                state = state * jnp.exp(last - base) + dot(vb, kd, ((0,), (0,)))
+                base = last
+            st[h, 0:dim, :] = state.astype(BF16)
+            st[h, dim:, :] = jnp.broadcast_to(jnp.exp(base), (st.shape[1] - dim, dim)).astype(BF16)
+            poll(1)
+
+    def state_copy(k):
+        return push(st, states.at[me], ss.at[k], sr.at[me], ep=k)
+
+    for k in range(1, eps):
+        @pl.when(ep_peer[k] > me)
+        def _():
+            state_copy(k).start()
+
+    def finish_mixer():
+        @pl.loop(0, me)
+        def _(hop):
+            pltpu.make_async_remote_copy(src_ref=st, dst_ref=states.at[hop], send_sem=ss.at[0], recv_sem=sr.at[hop],
+                                         device_id={"ep": hop}, device_id_type=MESH).wait_recv()
+
+        for h in range(heads):
+            c = slice(h * dim, (h + 1) * dim)
+
+            def one(hop, state):
+                own = states[hop, h, 0:dim, :].astype(F32)
+                passing = states[hop, h, dim:dim + 16, :].astype(F32)[0:1]
+                return state * passing + own
+
+            state = lax.fori_loop(0, me, one, jnp.zeros((dim, dim), F32))
+            out = lo[:, c] + dot(qd[:, c], state.astype(BF16), ((1,), (1,)))
+            scale = lax.rsqrt(jnp.mean(out * out, axis=1, keepdims=True) + epsilon)
+            gated[:, c] = (out * scale * hgain_ref[...].astype(F32) * og[:, c]).astype(BF16)
+        loads[7].wait()
+        for r in (3, 1, 2, 0):
+            block = wm[:, pl.ds(pl.multiple_of(tp_peer[r] * cols, cols), cols)]
+            mixed[r] = dot(gated[...], block).astype(BF16)
+            if r:
+                go(push(mixed.at[r], mixin.at[r], ms.at[r], mr.at[r], tp=r))
+
+    tile = 256 if units % 256 == 0 else units
+    chunks = eps // GROUPS
+    grows = chunks * cap
+
+    def feed(group):
+        for i in range(chunks):
+            k = group * chunks + i
+            complete(k)
+            r = slice(k * cap, (k + 1) * cap)
+            squares = jnp.zeros((cap, 1), F32)
+            for p in range(tps):
+                v = gath[p, r, :].astype(F32)
+                squares += jnp.sum(v * v, axis=1, keepdims=True)
+            scale = lax.rsqrt(squares / depth + epsilon)
+            for p in range(tps):
+                c = slice(p * cols, (p + 1) * cols)
+                enormed[r, c] = (gath[p, r, :].astype(F32) * scale * egain_ref[:, c].astype(F32)).astype(BF16)
+
+    def upward(group):
+        r = slice(group * grows, (group + 1) * grows)
+        for u in range(units // tile):
+            c = slice(u * tile, (u + 1) * tile)
+            gate = dot(enormed[r, :], wg[:, c])
+            up = dot(enormed[r, :], wu[:, c])
+            hidden[:, c] = (gate * sigmoid(gate) * up).astype(BF16)
+            poll(1)
+
+    def downward(group):
+        r = slice(group * grows, (group + 1) * grows)
+        for t in (3, 1, 2, 0):
+            block = wd[:, pl.ds(pl.multiple_of(tp_peer[t] * cols, cols), cols)]
+            psend[t, r, :] = dot(hidden[...], block).astype(BF16)
+            if t:
+                go(push(psend.at[t, r], precv.at[t, r], ps.at[group, t], pr.at[group, t], tp=t))
+
+    def reduce(group):
+        r = slice(group * grows, (group + 1) * grows)
+        for t in range(1, tps):
+            push(psend.at[t, r], precv.at[t, r], ps.at[group, t], pr.at[group, t], tp=t).wait_recv()
+        for i in range(chunks):
+            k = group * chunks + i
+            r = slice(k * cap, (k + 1) * cap)
+            value = psend[0, r, :].astype(F32)
+            for t in range(1, tps):
+                value += precv[t, r, :].astype(F32)
+            if k:
+                esum[r, :] = value.astype(BF16)
+                go(push(esum.at[r], back.at[r], bs.at[k], br.at[k], ep=k))
+            else:
+                back[r, :] = value.astype(BF16)
+
+    scores = scores_ref[...]
+    weights = scores / jnp.sum(scores, axis=1, keepdims=True)
+
+    def combine_group(group):
+        for i in range(chunks):
+            k = group * chunks + i
+            if k:
+                r = slice(k * cap, (k + 1) * cap)
+                push(esum.at[r], back.at[r], bs.at[k], br.at[k], ep=k).wait_recv()
+        r = slice(group * grows, (group + 1) * grows)
+        value = jnp.zeros((length, cols), F32)
+        for j in range(hits.shape[0]):
+            value += dot(hits[j, :, r], back[r, :]) * weights[:, j:j + 1]
+        return value
+
+    for load in loads[4:7]:
+        load.wait()
+    while len(agenda) > 3 * 2:
+        poll(1)
+    feed(0)
+    upward(0)
+    downward(0)
+    poll(len(agenda))
+    feed(1)
+    upward(1)
+    downward(1)
+    finish_mixer()
+    reduce(0)
+    total[...] = combine_group(0)
+    reduce(1)
+    for r in range(1, tps):
+        push(mixed.at[r], mixin.at[r], ms.at[r], mr.at[r], tp=r).wait_recv()
+    value = mixed[0].astype(F32)
+    for r in range(1, tps):
+        value += mixin[r].astype(F32)
+    mix_out[...] = value.astype(BF16)
+    moe_out[...] = (total[...] + combine_group(1)).astype(BF16)
+
+    for copy in sent:
+        copy.wait_send()
+    for k in range(1, eps):
+        @pl.when(ep_peer[k] > me)
+        def _():
+            state_copy(k).wait_send()
+
+
+def whole_block(mix_rows, mix_gain, wq, wf, wi, wo, gap, dec, hgain, wm, moe_rows, moe_gain, ids, scores, wg, wu, wd):
+    eps, tps = lax.axis_size("ep"), lax.axis_size("tp")
+    length, cols = mix_rows.shape
+    top = ids.shape[1]
+    cap = length * top * 3 // (2 * eps)
+    rows = eps * cap
+    heads = dec.shape[0]
+    width = wq.shape[1]
+    dim = width // heads
+    depth, units = wg.shape[1:]
+    dma = lambda *s: pltpu.SemaphoreType.DMA(s)
+    out = jax.ShapeDtypeStruct((length, cols), BF16)
+    scratch = [
+        pltpu.VMEM((4, depth, width), BF16), pltpu.VMEM((width, depth), BF16),
+        pltpu.VMEM((depth, units), BF16), pltpu.VMEM((depth, units), BF16), pltpu.VMEM((units, depth), BF16),
+        pltpu.VMEM((tps, length, cols), BF16), pltpu.VMEM((length, depth), BF16),
+        pltpu.VMEM((length, width), F32), pltpu.VMEM((length, width), BF16), pltpu.VMEM((length, width), F32),
+        pltpu.VMEM((heads, dim + 16, dim), BF16), pltpu.VMEM((eps, heads, dim + 16, dim), BF16),
+        pltpu.VMEM((length, width), BF16), pltpu.VMEM((tps, length, cols), BF16), pltpu.VMEM((tps, length, cols), BF16),
+        pltpu.VMEM((tps, rows, cols), BF16), pltpu.VMEM((rows, cols), BF16), pltpu.VMEM((top, length, rows), BF16),
+        pltpu.VMEM((rows, depth), BF16), pltpu.VMEM((rows // GROUPS, units), BF16),
+        pltpu.VMEM((tps, rows, cols), BF16), pltpu.VMEM((tps, rows, cols), BF16),
+        pltpu.VMEM((rows, cols), BF16), pltpu.VMEM((rows, cols), BF16), pltpu.VMEM((length, cols), F32),
+        dma(8), dma(4), dma(4), dma(eps), dma(eps), dma(eps, 4), dma(eps, 4), dma(GROUPS, tps), dma(GROUPS, tps),
+        dma(eps), dma(eps), dma(eps), dma(eps), dma(tps), dma(tps),
+    ]
+    return pl.pallas_call(
+        functools.partial(block_kernel, cap),
+        in_specs=[VMEM, VMEM, ANY, ANY, ANY, ANY, VMEM, VMEM, VMEM, ANY, VMEM, VMEM, VMEM, VMEM, ANY, ANY, ANY],
+        out_specs=[VMEM, VMEM],
+        out_shape=[out, out],
+        scratch_shapes=scratch,
+        compiler_params=pltpu.CompilerParams(vmem_limit_bytes=LIMIT, collective_id=0, has_side_effects=True),
+    )(mix_rows, mix_gain.reshape(1, -1), wq, wf, wi, wo, gap.reshape(1, -1), dec, hgain.reshape(1, -1), wm,
+      moe_rows, moe_gain.reshape(1, -1), ids, scores, wg, wu, wd)
+
+
+def fits(eps, tps, mix_rows, dec, route_ids, w_gate):
+    tokens, cols = mix_rows.shape
+    top = route_ids.shape[1]
+    cap = tokens * top * 3 // (2 * eps)
+    square = tps == 4 and eps >= 2 and eps & (eps - 1) == 0
+    aligned = cap % 32 == 0 and cols % 128 == 0 and tokens % (2 * BLOCK) == 0 and w_gate.shape[2] % 128 == 0
+    return square and aligned and w_gate.shape[0] == 1
+
 
 def per_device(mix_rows, mix_gain, w_query, w_forget, w_input, w_outgate, forget_gap, decay_extra,
                head_gain, w_mixout, moe_rows, moe_gain, route_ids, route_scores, w_gate, w_up, w_down):
     eps, tps = lax.axis_size("ep"), lax.axis_size("tp")
+    if fits(eps, tps, mix_rows, decay_extra, route_ids, w_gate):
+        return whole_block(mix_rows, mix_gain, w_query, w_forget, w_input, w_outgate, forget_gap, decay_extra,
+                           head_gain, w_mixout, moe_rows, moe_gain, route_ids, route_scores, w_gate, w_up, w_down)
     tokens, top = route_ids.shape
     experts = w_gate.shape[0] * eps
     capacity = tokens * top * 3 // (2 * experts)

time: 195 us -> 112 us (0.57)
  the two profiles are of different devices: /device:TPU:0 before, /device:TPU:9 now
where the time goes in v1:
time: 112 us
  Pallas kernels  102 us (91%)
  local copies, waits for them, and re-layouts  8.86 us (8%)
    pallas_call x1, Pallas kernels, whole_block(): pl.pallas_call(functools.partial(block_kernel, cap), in_specs=[VMEM, VMEM...  102 us
    unnamed x4, local copies, waits for them, and re-layouts  6.29 us

profile of v1, /device:TPU:9, one launch (start us, length us, event | category | flops | bytes accessed | tf_op | source)
XLA Modules:
  0.0 112.0 jit_solution(8980502948286548191)
XLA Ops:
  0.6 1.3 %reshape.16.mgain_ref = bf16[1,2048]{1,0:T(2,128)(2,1)} reshape(bf16[2048]{0:T(1024)(128)(2,1)} %param.18) | data formatting | bytes 8192 | tf_op jit(solution)/shard_map/reshape | solution.py:604
  1.9 1.3 %reshape.19.egain_ref = bf16[1,2048]{1,0:T(2,128)(2,1)} reshape(bf16[2048]{0:T(1024)(128)(2,1)} %param.28) | data formatting | bytes 8192 | tf_op jit(solution)/shard_map/reshape | solution.py:605
  3.2 1.5 %copy.19.ids_ref = s32[256,2]{1,0:T(8,128)} copy(s32[256,2]{0,1:T(2,128)} %param.29) | data formatting | bytes 4096 | tf_op args[12]
  4.7 1.5 %copy.20.scores_ref = f32[256,2]{1,0:T(8,128)} copy(f32[256,2]{0,1:T(2,128)} %param.30) | data formatting | bytes 4096 | tf_op args[13]
  6.2 102.5 %shard_map.176 = (bf16[256,512]{1,0:T(8,128)(2,1)}, bf16[256,512]{1,0:T(8,128)(2,1)}) custom-call(bf16[256,512]{1,0:T(8,128)(2,1)} %mix_ref.1, bf16[1,2048]{1,0:T(2,128)(2,1)} %reshape.16.mgain_ref, bf16[2048,512]{1,0:T(8,128)(2,1)} %wq_hbm.1, bf16[2048,512]{1,0:T(8,128)(2,1)} %wf_hbm.1, bf16[2048,512]{1,0:T(8,128)(2,1)} %wi_hbm.1, ...), custom_call_target="tpu_custom_call" | custom-call | tf_op jit(solution)/shard_map/pallas_call | solution.py:597
  108.6 1.7 %copy.23 = bf16[256,512]{1,0:T(8,128)(2,1)} copy(bf16[256,512]{1,0:T(8,128)(2,1)} %get-tuple-element.4) | data formatting | bytes 524288
  110.3 1.7 %copy.24 = bf16[256,512]{1,0:T(8,128)(2,1)} copy(bf16[256,512]{1,0:T(8,128)(2,1)} %get-tuple-element.5) | data formatting | bytes 524288

commit v2 on v1

--- a/solution.py
+++ b/solution.py
@@ -256,6 +256,7 @@
 ANY = pl.BlockSpec(memory_space=pl.ANY)
 HIGHEST = lax.Precision.HIGHEST
 GROUPS = 2
+PAIR = 2
 
 
 def flip(place, bits):
@@ -267,10 +268,10 @@
     return place
 
 
-def block_kernel(cap, mix_ref, mgain_ref, wq_hbm, wf_hbm, wi_hbm, wo_hbm, gap_ref, dec_ref, hgain_ref, wm_hbm,
-                 moe_ref, egain_ref, ids_ref, scores_ref, wg_hbm, wu_hbm, wd_hbm,
+def block_kernel(cap, mix_hbm, mgain_ref, wq_hbm, wf_hbm, wi_hbm, wo_hbm, gap_ref, dec_ref, hgain_ref, wm_hbm,
+                 moe_hbm, egain_ref, ids_ref, scores_ref, wg_hbm, wu_hbm, wd_hbm,
                  mix_out, moe_out,
-                 wmix, wm, wg, wu, wd, xall, normed, lo, qd, og, st, states, gated, mixed, mixin,
+                 mix_ref, moe_ref, wmix, wm, wg, wu, wd, xall, normed, lo, qd, og, st, pst, cst, states, gated, mixed, mixin,
                  gath, slots, hits, enormed, hidden, psend, precv, esum, back, total,
                  wsem, xs, xr, zs, zr, gs, gr, ps, pr, bs, br, ss, sr, ms, mr):
     eps, tps = lax.axis_size("ep"), lax.axis_size("tp")
@@ -297,14 +298,16 @@
     loads = [pltpu.make_async_copy(s, wmix.at[i], wsem.at[i]) for i, s in enumerate((wq_hbm, wf_hbm, wi_hbm, wo_hbm))]
     loads += [pltpu.make_async_copy(wg_hbm.at[0], wg, wsem.at[4]), pltpu.make_async_copy(wu_hbm.at[0], wu, wsem.at[5]),
               pltpu.make_async_copy(wd_hbm.at[0], wd, wsem.at[6]), pltpu.make_async_copy(wm_hbm, wm, wsem.at[7])]
-    for load in loads:
-        load.start()
+    rowload = [pltpu.make_async_copy(mix_hbm, mix_ref, wsem.at[8]), pltpu.make_async_copy(moe_hbm, moe_ref, wsem.at[9])]
 
     barrier = pltpu.get_barrier_semaphore()
     for k in range(1, eps):
         pl.semaphore_signal(barrier, inc=1, device_id={"ep": ep_peer[k]}, device_id_type=MESH)
     for r in range(1, tps):
         pl.semaphore_signal(barrier, inc=1, device_id={"tp": tp_peer[r]}, device_id_type=MESH)
+    for load in rowload + loads:
+        load.start()
+    rowload[0].wait()
     pl.semaphore_wait(barrier, eps + tps - 2)
 
     half = length // 2
@@ -313,12 +316,14 @@
 
     experts = eps
     names = iota((length, experts), 1)
-    ids = ids_ref[...]
+    eye = iota((length, length), 0) == iota((length, length), 1)
+    ids = dot(eye.astype(BF16), ids_ref[...].astype(F32).astype(BF16), ((1,), (1,))).astype(jnp.int32)
     picks = [ids[:, j:j + 1] == names for j in range(ids.shape[1])]
     chosen = functools.reduce(jnp.logical_or, picks)
     before = (iota((length, length), 0) > iota((length, length), 1)).astype(BF16)
     rank = dot(before, chosen.astype(BF16)).astype(jnp.int32)
     spot = rank + jnp.bitwise_xor(names, me) * cap
+    rowload[1].wait()
     both = None
     for j, pick in enumerate(picks):
         at = jnp.sum(jnp.where(pick, spot, 0), axis=1, keepdims=True)
@@ -385,9 +390,13 @@
         v = xall[p].astype(F32)
         squares += jnp.sum(v * v, axis=1, keepdims=True)
     scale = lax.rsqrt(squares / depth + epsilon)
+    mgain, egain = mgain_ref[...].astype(F32), egain_ref[...].astype(F32)
+    lanes = mgain.shape[1]
     for p in range(tps):
-        c = slice(p * cols, (p + 1) * cols)
-        normed[:, c] = (xall[p].astype(F32) * scale * mgain_ref[:, c].astype(F32)).astype(BF16)
+        for i in range(cols // lanes):
+            s = slice(i * lanes, (i + 1) * lanes)
+            n = p * (cols // lanes) + i
+            normed[:, n * lanes:(n + 1) * lanes] = (xall[p, :, s].astype(F32) * scale * mgain[n:n + 1]).astype(BF16)
     poll(1)
 
     tri = (iota((length, length), 0) >= iota((length, length), 1)).astype(F32)
@@ -438,19 +447,33 @@
             st[h, dim:, :] = jnp.broadcast_to(jnp.exp(base), (st.shape[1] - dim, dim)).astype(BF16)
             poll(1)
 
-    def state_copy(k):
-        return push(st, states.at[me], ss.at[k], sr.at[me], ep=k)
-
-    for k in range(1, eps):
-        @pl.when(ep_peer[k] > me)
-        def _():
-            state_copy(k).start()
+    odd = lax.rem(me, PAIR)
+    pair = lax.div(me, PAIR)
+    swap = push(st, pst, ss.at[1], sr.at[0], ep=1)
+    go(swap)
+
+    def joined_copy(k):
+        return push(cst, states.at[pair], ss.at[k], sr.at[1 + pair], ep=k)
+
+    def parts_of(ref, h):
+        return ref[h, 0:dim, :].astype(F32), ref[h, dim:dim + 16, :].astype(F32)[0:1]
+
+    def join_states():
+        swap.wait_recv()
+        for h in range(heads):
+            (own, keep), (other, pass_on) = parts_of(st, h), parts_of(pst, h)
+            cst[h, 0:dim, :] = jnp.where(odd == 1, other * keep + own, own * pass_on + other).astype(BF16)
+            cst[h, dim:, :] = jnp.broadcast_to(keep * pass_on, (st.shape[1] - dim, dim)).astype(BF16)
+        for k in range(PAIR, eps, PAIR):
+            @pl.when(ep_peer[k] > me)
+            def _():
+                joined_copy(k).start()
 
     def finish_mixer():
-        @pl.loop(0, me)
+        @pl.loop(0, pair)
         def _(hop):
-            pltpu.make_async_remote_copy(src_ref=st, dst_ref=states.at[hop], send_sem=ss.at[0], recv_sem=sr.at[hop],
-                                         device_id={"ep": hop}, device_id_type=MESH).wait_recv()
+            pltpu.make_async_remote_copy(src_ref=cst, dst_ref=states.at[hop], send_sem=ss.at[0], recv_sem=sr.at[1 + hop],
+                                         device_id={"ep": hop * PAIR + odd}, device_id_type=MESH).wait_recv()
 
         for h in range(heads):
             c = slice(h * dim, (h + 1) * dim)
@@ -460,7 +483,9 @@
                 passing = states[hop, h, dim:dim + 16, :].astype(F32)[0:1]
                 return state * passing + own
 
-            state = lax.fori_loop(0, me, one, jnp.zeros((dim, dim), F32))
+            state = lax.fori_loop(0, pair, one, jnp.zeros((dim, dim), F32))
+            other, pass_on = parts_of(pst, h)
+            state = jnp.where(odd == 1, state * pass_on + other, state)
             out = lo[:, c] + dot(qd[:, c], state.astype(BF16), ((1,), (1,)))
             scale = lax.rsqrt(jnp.mean(out * out, axis=1, keepdims=True) + epsilon)
             gated[:, c] = (out * scale * hgain_ref[...].astype(F32) * og[:, c]).astype(BF16)
@@ -468,8 +493,6 @@
         for r in (3, 1, 2, 0):
             block = wm[:, pl.ds(pl.multiple_of(tp_peer[r] * cols, cols), cols)]
             mixed[r] = dot(gated[...], block).astype(BF16)
-            if r:
-                go(push(mixed.at[r], mixin.at[r], ms.at[r], mr.at[r], tp=r))
 
     tile = 256 if units % 256 == 0 else units
     chunks = eps // GROUPS
@@ -486,8 +509,11 @@
                 squares += jnp.sum(v * v, axis=1, keepdims=True)
             scale = lax.rsqrt(squares / depth + epsilon)
             for p in range(tps):
-                c = slice(p * cols, (p + 1) * cols)
-                enormed[r, c] = (gath[p, r, :].astype(F32) * scale * egain_ref[:, c].astype(F32)).astype(BF16)
+                for i in range(cols // lanes):
+                    s = slice(i * lanes, (i + 1) * lanes)
+                    n = p * (cols // lanes) + i
+                    c = slice(n * lanes, (n + 1) * lanes)
+                    enormed[r, c] = (gath[p, r, s].astype(F32) * scale * egain[n:n + 1]).astype(BF16)
 
     def upward(group):
         r = slice(group * grows, (group + 1) * grows)
@@ -503,69 +529,111 @@
         for t in (3, 1, 2, 0):
             block = wd[:, pl.ds(pl.multiple_of(tp_peer[t] * cols, cols), cols)]
             psend[t, r, :] = dot(hidden[...], block).astype(BF16)
-            if t:
-                go(push(psend.at[t, r], precv.at[t, r], ps.at[group, t], pr.at[group, t], tp=t))
-
-    def reduce(group):
-        r = slice(group * grows, (group + 1) * grows)
-        for t in range(1, tps):
-            push(psend.at[t, r], precv.at[t, r], ps.at[group, t], pr.at[group, t], tp=t).wait_recv()
-        for i in range(chunks):
-            k = group * chunks + i
-            r = slice(k * cap, (k + 1) * cap)
-            value = psend[0, r, :].astype(F32)
-            for t in range(1, tps):
-                value += precv[t, r, :].astype(F32)
+
+    def summing(src, dst, a, b, send, recv):
+        def part(n, index, target, r, tp):
+            return push(src.at[index, r], dst.at[target, r], send.at[n], recv.at[n], tp=tp)
+
+        first = [part(0, 3, 3, a, 1), part(1, 3, 3, b, 2), part(2, 1, 1, a, 1), part(3, 2, 2, b, 2)]
+        second = [part(4, 2, 2, a, 2), part(5, 1, 1, b, 1)]
+
+        def start():
+            for copy in first:
+                go(copy)
+
+        def merge():
+            first[0].wait_recv()
+            src[2, a, :] = (src[2, a, :].astype(F32) + dst[3, a, :].astype(F32)).astype(BF16)
+            first[1].wait_recv()
+            src[1, b, :] = (src[1, b, :].astype(F32) + dst[3, b, :].astype(F32)).astype(BF16)
+            for copy in second:
+                go(copy)
+
+        def finish():
+            for copy in first[2:] + second:
+                copy.wait_recv()
+
+        def value(r):
+            return src[0, r, :].astype(F32) + dst[1, r, :].astype(F32) + dst[2, r, :].astype(F32)
+
+        return start, merge, finish, value
+
+    def chunk(k):
+        return slice(k * cap, (k + 1) * cap)
+
+    sums = [summing(psend, precv, chunk(2 * g), chunk(2 * g + 1), ps.at[g], pr.at[g]) for g in range(eps // 2)]
+    mixsum = summing(mixed, mixin, slice(0, half), slice(half, length), ms, mr)
+
+    def give_back(g):
+        _, _, finish, value = sums[g]
+        finish()
+        for k in (2 * g, 2 * g + 1):
+            r = chunk(k)
             if k:
-                esum[r, :] = value.astype(BF16)
+                esum[r, :] = value(r).astype(BF16)
                 go(push(esum.at[r], back.at[r], bs.at[k], br.at[k], ep=k))
             else:
-                back[r, :] = value.astype(BF16)
+                back[r, :] = value(r).astype(BF16)
 
     scores = scores_ref[...]
-    weights = scores / jnp.sum(scores, axis=1, keepdims=True)
-
-    def combine_group(group):
-        for i in range(chunks):
-            k = group * chunks + i
+    weights = dot(eye.astype(F32), scores / jnp.sum(scores, axis=0, keepdims=True), ((1,), (1,)), precision=HIGHEST)
+
+    def combine(g):
+        for k in (2 * g, 2 * g + 1):
             if k:
-                r = slice(k * cap, (k + 1) * cap)
-                push(esum.at[r], back.at[r], bs.at[k], br.at[k], ep=k).wait_recv()
-        r = slice(group * grows, (group + 1) * grows)
+                push(esum.at[chunk(k)], back.at[chunk(k)], bs.at[k], br.at[k], ep=k).wait_recv()
+        r = slice(2 * g * cap, (2 * g + 2) * cap)
         value = jnp.zeros((length, cols), F32)
         for j in range(hits.shape[0]):
             value += dot(hits[j, :, r], back[r, :]) * weights[:, j:j + 1]
         return value
 
+    far = list(range(eps // 2 - 1, eps // 4 - 1, -1))
+    near = list(range(eps // 4 - 1, 0, -1))
     for load in loads[4:7]:
         load.wait()
-    while len(agenda) > 3 * 2:
+    join_states()
+    while len(agenda) > eps:
         poll(1)
     feed(0)
     upward(0)
     downward(0)
     poll(len(agenda))
+    for g in near:
+        sums[g][0]()
     feed(1)
     upward(1)
+    for g in near:
+        sums[g][1]()
     downward(1)
+    for g in far:
+        sums[g][0]()
     finish_mixer()
-    reduce(0)
-    total[...] = combine_group(0)
-    reduce(1)
-    for r in range(1, tps):
-        push(mixed.at[r], mixin.at[r], ms.at[r], mr.at[r], tp=r).wait_recv()
-    value = mixed[0].astype(F32)
-    for r in range(1, tps):
-        value += mixin[r].astype(F32)
-    mix_out[...] = value.astype(BF16)
-    moe_out[...] = (total[...] + combine_group(1)).astype(BF16)
+    for g in far:
+        sums[g][1]()
+    mixsum[0]()
+    for g in near:
+        give_back(g)
+    sums[0][0]()
+    for g in far:
+        give_back(g)
+    mixsum[1]()
+    sums[0][1]()
+    value = None
+    for g in near + far:
+        value = combine(g) if value is None else value + combine(g)
+    total[...] = value
+    mixsum[2]()
+    mix_out[...] = mixsum[3](slice(0, length)).astype(BF16)
+    give_back(0)
+    moe_out[...] = (total[...] + combine(0)).astype(BF16)
 
     for copy in sent:
         copy.wait_send()
-    for k in range(1, eps):
+    for k in range(PAIR, eps, PAIR):
         @pl.when(ep_peer[k] > me)
         def _():
-            state_copy(k).wait_send()
+            joined_copy(k).wait_send()
 
 
 def whole_block(mix_rows, mix_gain, wq, wf, wi, wo, gap, dec, hgain, wm, moe_rows, moe_gain, ids, scores, wg, wu, wd):
@@ -581,35 +649,37 @@
     dma = lambda *s: pltpu.SemaphoreType.DMA(s)
     out = jax.ShapeDtypeStruct((length, cols), BF16)
     scratch = [
+        pltpu.VMEM((length, cols), BF16), pltpu.VMEM((length, cols), BF16),
         pltpu.VMEM((4, depth, width), BF16), pltpu.VMEM((width, depth), BF16),
         pltpu.VMEM((depth, units), BF16), pltpu.VMEM((depth, units), BF16), pltpu.VMEM((units, depth), BF16),
         pltpu.VMEM((tps, length, cols), BF16), pltpu.VMEM((length, depth), BF16),
         pltpu.VMEM((length, width), F32), pltpu.VMEM((length, width), BF16), pltpu.VMEM((length, width), F32),
-        pltpu.VMEM((heads, dim + 16, dim), BF16), pltpu.VMEM((eps, heads, dim + 16, dim), BF16),
+        pltpu.VMEM((heads, dim + 16, dim), BF16), pltpu.VMEM((heads, dim + 16, dim), BF16),
+        pltpu.VMEM((heads, dim + 16, dim), BF16), pltpu.VMEM((eps // PAIR, heads, dim + 16, dim), BF16),
         pltpu.VMEM((length, width), BF16), pltpu.VMEM((tps, length, cols), BF16), pltpu.VMEM((tps, length, cols), BF16),
         pltpu.VMEM((tps, rows, cols), BF16), pltpu.VMEM((rows, cols), BF16), pltpu.VMEM((top, length, rows), BF16),
         pltpu.VMEM((rows, depth), BF16), pltpu.VMEM((rows // GROUPS, units), BF16),
         pltpu.VMEM((tps, rows, cols), BF16), pltpu.VMEM((tps, rows, cols), BF16),
         pltpu.VMEM((rows, cols), BF16), pltpu.VMEM((rows, cols), BF16), pltpu.VMEM((length, cols), F32),
-        dma(8), dma(4), dma(4), dma(eps), dma(eps), dma(eps, 4), dma(eps, 4), dma(GROUPS, tps), dma(GROUPS, tps),
-        dma(eps), dma(eps), dma(eps), dma(eps), dma(tps), dma(tps),
+        dma(10), dma(4), dma(4), dma(eps), dma(eps), dma(eps, 4), dma(eps, 4), dma(eps // 2, 6), dma(eps // 2, 6),
+        dma(eps), dma(eps), dma(eps), dma(eps), dma(6), dma(6),
     ]
     return pl.pallas_call(
         functools.partial(block_kernel, cap),
-        in_specs=[VMEM, VMEM, ANY, ANY, ANY, ANY, VMEM, VMEM, VMEM, ANY, VMEM, VMEM, VMEM, VMEM, ANY, ANY, ANY],
+        in_specs=[ANY, VMEM, ANY, ANY, ANY, ANY, VMEM, VMEM, VMEM, ANY, ANY, VMEM, VMEM, VMEM, ANY, ANY, ANY],
         out_specs=[VMEM, VMEM],
         out_shape=[out, out],
         scratch_shapes=scratch,
         compiler_params=pltpu.CompilerParams(vmem_limit_bytes=LIMIT, collective_id=0, has_side_effects=True),
-    )(mix_rows, mix_gain.reshape(1, -1), wq, wf, wi, wo, gap.reshape(1, -1), dec, hgain.reshape(1, -1), wm,
-      moe_rows, moe_gain.reshape(1, -1), ids, scores, wg, wu, wd)
+    )(mix_rows, mix_gain.reshape(-1, 128), wq, wf, wi, wo, gap.reshape(1, -1), dec, hgain.reshape(1, -1), wm,
+      moe_rows, moe_gain.reshape(-1, 128), ids.T, scores.T, wg, wu, wd)
 
 
 def fits(eps, tps, mix_rows, dec, route_ids, w_gate):
     tokens, cols = mix_rows.shape
     top = route_ids.shape[1]
     cap = tokens * top * 3 // (2 * eps)
-    square = tps == 4 and eps >= 2 and eps & (eps - 1) == 0
+    square = tps == 4 and eps >= 4 and eps & (eps - 1) == 0
     aligned = cap % 32 == 0 and cols % 128 == 0 and tokens % (2 * BLOCK) == 0 and w_gate.shape[2] % 128 == 0
     return square and aligned and w_gate.shape[0] == 1
 

time: 112 us -> 86.2 us (0.77)
  the two profiles are of different devices: /device:TPU:9 before, /device:TPU:0 now
where the time goes in v2:
time: 86.2 us; the launch traced here: 85.7 us
  Pallas kernels  81.7 us (95%)
  local copies, waits for them, and re-layouts  3.34 us (4%)
    pallas_call x1, Pallas kernels, whole_block(): pl.pallas_call(functools.partial(block_kernel, cap), in_specs=[ANY, VMEM,...  81.7 us
    unnamed x2, local copies, waits for them, and re-layouts  3.34 us

profile of v2, /device:TPU:0, one launch (start us, length us, event | category | flops | bytes accessed | tf_op | source)
XLA Modules:
  0.0 85.7 jit_solution(6827033513290519006)
XLA Ops:
  0.6 81.7 %shard_map.176 = (bf16[256,512]{1,0:T(8,128)(2,1)}, bf16[256,512]{1,0:T(8,128)(2,1)}) custom-call(bf16[256,512]{1,0:T(8,128)(2,1)} %mix_hbm.1, bf16[16,128]{1,0:T(8,128)(2,1)} %bitcast.6, bf16[2048,512]{1,0:T(8,128)(2,1)} %wq_hbm.1, bf16[2048,512]{1,0:T(8,128)(2,1)} %wf_hbm.1, bf16[2048,512]{1,0:T(8,128)(2,1)} %wi_hbm.1, bf16[2048,512]{1,0:T(8,128)(2,1)} %wo_hbm.1, ...), custom_call_target="tpu_custom_call" | custom-call | tf_op jit(solution)/shard_map/pallas_call | solution.py:667
  82.4 1.7 %copy.21 = bf16[256,512]{1,0:T(8,128)(2,1)} copy(bf16[256,512]{1,0:T(8,128)(2,1)} %get-tuple-element.4) | data formatting | bytes 524288
  84.1 1.7 %copy.22 = bf16[256,512]{1,0:T(8,128)(2,1)} copy(bf16[256,512]{1,0:T(8,128)(2,1)} %get-tuple-element.5) | data formatting | bytes 524288

commit v3 on v2

--- a/solution.py
+++ b/solution.py
@@ -255,7 +255,6 @@
 MESH = pl.DeviceIdType.MESH
 ANY = pl.BlockSpec(memory_space=pl.ANY)
 HIGHEST = lax.Precision.HIGHEST
-GROUPS = 2
 PAIR = 2
 
 
@@ -271,9 +270,9 @@
 def block_kernel(cap, mix_hbm, mgain_ref, wq_hbm, wf_hbm, wi_hbm, wo_hbm, gap_ref, dec_ref, hgain_ref, wm_hbm,
                  moe_hbm, egain_ref, ids_ref, scores_ref, wg_hbm, wu_hbm, wd_hbm,
                  mix_out, moe_out,
-                 mix_ref, moe_ref, wmix, wm, wg, wu, wd, xall, normed, lo, qd, og, st, pst, cst, states, gated, mixed, mixin,
-                 gath, slots, hits, enormed, hidden, psend, precv, esum, back, total,
-                 wsem, xs, xr, zs, zr, gs, gr, ps, pr, bs, br, ss, sr, ms, mr):
+                 mix_ref, moe_ref, wmix, wm, wg, wu, wd, xall, acc, lo, qd, og, st, pst, cst, fst, states, gated, mixed, mixin,
+                 gath, slots, hits, enormed, hidden, psend, precv, nback, tok, tokin, esum, back, total,
+                 wsem, xs, xr, zs, zr, gs, gr, ps, pr, bs, br, ss, sr, ms, mr, ts, tr):
     eps, tps = lax.axis_size("ep"), lax.axis_size("tp")
     me, mt = lax.axis_index("ep"), lax.axis_index("tp")
     length, cols = mix_ref.shape
@@ -373,30 +372,52 @@
             ref = xall.at[tp_peer[3], pl.ds(n * half, half)]
             push(ref, ref, xs.at[2 + n], xr.at[2 + n], tp=via).wait_recv()
 
-    agenda = [functools.partial(spread, 0), relay_mix, functools.partial(spread, 1), functools.partial(relay, 0)]
-    for k in range(2, eps):
-        agenda += [functools.partial(spread, k), functools.partial(relay, k - 1)]
-    agenda.append(functools.partial(relay, eps - 1))
+    S, R = (lambda k: functools.partial(spread, k)), (lambda k: functools.partial(relay, k))
+    agenda = []
+    for k in range(1, eps):
+        agenda += [S(k + 2), R(k)] if k + 2 < eps else [R(k)]
+    spot = 2 * (eps // 2 - 1) - 1
+    if eps // 2 + 1 < eps:
+        agenda[spot - 1:spot + 1] = agenda[spot - 1:spot + 1][::-1]
+    near_end = len(agenda) - spot if eps // 2 + 1 < eps else 0
 
     def poll(count=1):
         for _ in range(min(count, len(agenda))):
             agenda.pop(0)()
 
-    poll(4)
-    xall[mt] = mix_ref[...]
-    complete_mix()
-    squares = jnp.zeros((length, 1), F32)
-    for p in range(tps):
-        v = xall[p].astype(F32)
-        squares += jnp.sum(v * v, axis=1, keepdims=True)
-    scale = lax.rsqrt(squares / depth + epsilon)
     mgain, egain = mgain_ref[...].astype(F32), egain_ref[...].astype(F32)
     lanes = mgain.shape[1]
-    for p in range(tps):
-        for i in range(cols // lanes):
-            s = slice(i * lanes, (i + 1) * lanes)
-            n = p * (cols // lanes) + i
-            normed[:, n * lanes:(n + 1) * lanes] = (xall[p, :, s].astype(F32) * scale * mgain[n:n + 1]).astype(BF16)
+    per_shard = cols // lanes
+    squares = [jnp.zeros((length, 1), F32)]
+
+    def project(r, ref, first):
+        p = tp_peer[r]
+        v = ref[...].astype(F32)
+        squares[0] += jnp.sum(v * v, axis=1, keepdims=True)
+        gains = mgain[0:per_shard]
+        for i in range(1, tps):
+            gains = jnp.where(p == i, mgain[i * per_shard:(i + 1) * per_shard], gains)
+        v = jnp.concatenate([v[:, i * lanes:(i + 1) * lanes] * gains[i:i + 1] for i in range(per_shard)], axis=1)
+        v = v.astype(BF16)
+        w = pl.ds(pl.multiple_of(p * cols, cols), cols)
+        for i in range(4):
+            part = dot(v, wmix[i, w, :])
+            acc[i] = part if first else acc[i] + part
+
+    S(0)()
+    for load in loads[:4]:
+        load.wait()
+    project(0, mix_ref, True)
+    relay_mix()
+    S(1)()
+    project(1, xall.at[tp_peer[1]], False)
+    R(0)()
+    S(2)()
+    project(2, xall.at[tp_peer[2]], False)
+    complete_mix()
+    poll(1)
+    project(3, xall.at[tp_peer[3]], False)
+    scale = lax.rsqrt(squares[0] / depth + epsilon)
     poll(1)
 
     tri = (iota((length, length), 0) >= iota((length, length), 1)).astype(F32)
@@ -404,20 +425,15 @@
     causal = iota((BLOCK, BLOCK), 0) >= iota((BLOCK, BLOCK), 1)
     mid = BLOCK // 2
     per = 2 if heads % 2 == 0 else 1
-    for load in loads[:4]:
-        load.wait()
-    for step in range(heads // per):
+
+    def mix_step(step):
         w = slice(step * per * dim, (step + 1) * per * dim)
-        n = normed[...]
-        qp = dot(n, wmix[0, :, w])
-        fp = dot(n, wmix[1, :, w])
-        value = dot(n, wmix[2, :, w]).astype(BF16)
-        op = dot(n, wmix[3, :, w])
+        qp, fp, value, op = [acc[i, :, w] * scale for i in range(4)]
+        value = value.astype(BF16)
         query = qp * sigmoid(qp)
         key = gap_ref[:, w] * sigmoid(-fp)
         og[:, w] = op * sigmoid(op)
         logs = jnp.log1p(-key)
-        poll(1)
         for j in range(per):
             h = step * per + j
             cl = slice(j * dim, (j + 1) * dim)
@@ -450,7 +466,9 @@
     odd = lax.rem(me, PAIR)
     pair = lax.div(me, PAIR)
     swap = push(st, pst, ss.at[1], sr.at[0], ep=1)
-    go(swap)
+    own_half = pl.ds(odd * (heads // 2), heads // 2)
+    other_half = pl.ds((1 - odd) * (heads // 2), heads // 2)
+    trade = push(fst.at[own_half], fst.at[own_half], ss.at[0], sr.at[eps - 1], ep=1)
 
     def joined_copy(k):
         return push(cst, states.at[pair], ss.at[k], sr.at[1 + pair], ep=k)
@@ -460,30 +478,36 @@
 
     def join_states():
         swap.wait_recv()
-        for h in range(heads):
+        for i in range(heads // 2):
+            h = odd * (heads // 2) + i
             (own, keep), (other, pass_on) = parts_of(st, h), parts_of(pst, h)
-            cst[h, 0:dim, :] = jnp.where(odd == 1, other * keep + own, own * pass_on + other).astype(BF16)
-            cst[h, dim:, :] = jnp.broadcast_to(keep * pass_on, (st.shape[1] - dim, dim)).astype(BF16)
+            cst[i, 0:dim, :] = jnp.where(odd == 1, other * keep + own, own * pass_on + other).astype(BF16)
+            cst[i, dim:, :] = jnp.broadcast_to(keep * pass_on, (st.shape[1] - dim, dim)).astype(BF16)
         for k in range(PAIR, eps, PAIR):
             @pl.when(ep_peer[k] > me)
             def _():
                 joined_copy(k).start()
 
-    def finish_mixer():
+    def fold_states():
         @pl.loop(0, pair)
         def _(hop):
             pltpu.make_async_remote_copy(src_ref=cst, dst_ref=states.at[hop], send_sem=ss.at[0], recv_sem=sr.at[1 + hop],
                                          device_id={"ep": hop * PAIR + odd}, device_id_type=MESH).wait_recv()
 
+        for i in range(heads // 2):
+            def one(hop, state):
+                own, pass_on = parts_of(states.at[hop], i)
+                return state * pass_on + own
+
+            state = lax.fori_loop(0, pair, one, jnp.zeros((dim, dim), F32))
+            fst[odd * (heads // 2) + i] = state.astype(BF16)
+        go(trade)
+
+    def finish_mixer():
+        push(fst.at[other_half], fst.at[other_half], ss.at[0], sr.at[eps - 1], ep=1).wait_recv()
         for h in range(heads):
             c = slice(h * dim, (h + 1) * dim)
-
-            def one(hop, state):
-                own = states[hop, h, 0:dim, :].astype(F32)
-                passing = states[hop, h, dim:dim + 16, :].astype(F32)[0:1]
-                return state * passing + own
-
-            state = lax.fori_loop(0, pair, one, jnp.zeros((dim, dim), F32))
+            state = fst[h].astype(F32)
             other, pass_on = parts_of(pst, h)
             state = jnp.where(odd == 1, state * pass_on + other, state)
             out = lo[:, c] + dot(qd[:, c], state.astype(BF16), ((1,), (1,)))
@@ -495,14 +519,12 @@
             mixed[r] = dot(gated[...], block).astype(BF16)
 
     tile = 256 if units % 256 == 0 else units
-    chunks = eps // GROUPS
-    grows = chunks * cap
-
-    def feed(group):
-        for i in range(chunks):
-            k = group * chunks + i
+    def feed(chunks, polls=()):
+        for k in chunks:
+            if k in polls:
+                poll(1)
             complete(k)
-            r = slice(k * cap, (k + 1) * cap)
+            r = chunk(k)
             squares = jnp.zeros((cap, 1), F32)
             for p in range(tps):
                 v = gath[p, r, :].astype(F32)
@@ -515,20 +537,29 @@
                     c = slice(n * lanes, (n + 1) * lanes)
                     enormed[r, c] = (gath[p, r, s].astype(F32) * scale * egain[n:n + 1]).astype(BF16)
 
-    def upward(group):
-        r = slice(group * grows, (group + 1) * grows)
+    def chunk(k):
+        return slice(k * cap, (k + 1) * cap)
+
+    def span(chunks):
+        return slice(chunks[0] * cap, (chunks[-1] + 1) * cap)
+
+    def upward(chunks, polls=()):
+        r = span(chunks)
         for u in range(units // tile):
             c = slice(u * tile, (u + 1) * tile)
             gate = dot(enormed[r, :], wg[:, c])
             up = dot(enormed[r, :], wu[:, c])
-            hidden[:, c] = (gate * sigmoid(gate) * up).astype(BF16)
-            poll(1)
-
-    def downward(group):
-        r = slice(group * grows, (group + 1) * grows)
+            hidden[0:len(chunks) * cap, c] = (gate * sigmoid(gate) * up).astype(BF16)
+            if u in polls:
+                poll(1)
+
+    def downward(chunks, polls=()):
+        r = span(chunks)
         for t in (3, 1, 2, 0):
             block = wd[:, pl.ds(pl.multiple_of(tp_peer[t] * cols, cols), cols)]
-            psend[t, r, :] = dot(hidden[...], block).astype(BF16)
+            psend[t, r, :] = dot(hidden[0:len(chunks) * cap, :], block).astype(BF16)
+            if t in polls:
+                poll(1)
 
     def summing(src, dst, a, b, send, recv):
         def part(n, index, target, r, tp):
@@ -558,75 +589,91 @@
 
         return start, merge, finish, value
 
-    def chunk(k):
-        return slice(k * cap, (k + 1) * cap)
-
-    sums = [summing(psend, precv, chunk(2 * g), chunk(2 * g + 1), ps.at[g], pr.at[g]) for g in range(eps // 2)]
+    near = list(range(eps // 2))
+    far = [[k, k + 1] for k in range(eps // 2, eps, 2)]
+    nrows = len(near) * cap
+    sums = [summing(psend, precv, chunk(a), chunk(b), ps.at[g], pr.at[g]) for g, (a, b) in enumerate(far)]
     mixsum = summing(mixed, mixin, slice(0, half), slice(half, length), ms, mr)
-
-    def give_back(g):
+    toksum = summing(tok, tokin, slice(0, half), slice(half, length), ts, tr)
+
+    def near_copy(k):
+        return push(psend.at[:, chunk(k)], nback.at[:, chunk(k)], bs.at[k], br.at[k], ep=k)
+
+    def give_near():
+        for k in near[1:]:
+            go(near_copy(k))
+        nback[:, chunk(0), :] = psend[:, chunk(0), :]
+
+    def take_near():
+        for k in near[1:]:
+            near_copy(k).wait_recv()
+        for t in (3, 1, 2, 0):
+            value = jnp.zeros((length, cols), F32)
+            for j in range(hits.shape[0]):
+                value += dot(hits[j, :, 0:nrows], nback[t]) * weights[:, j:j + 1]
+            tok[t] = value.astype(BF16)
+
+    def give_far(g):
         _, _, finish, value = sums[g]
         finish()
-        for k in (2 * g, 2 * g + 1):
+        for k in far[g]:
             r = chunk(k)
-            if k:
-                esum[r, :] = value(r).astype(BF16)
-                go(push(esum.at[r], back.at[r], bs.at[k], br.at[k], ep=k))
-            else:
-                back[r, :] = value(r).astype(BF16)
-
-    scores = scores_ref[...]
-    weights = dot(eye.astype(F32), scores / jnp.sum(scores, axis=0, keepdims=True), ((1,), (1,)), precision=HIGHEST)
-
-    def combine(g):
-        for k in (2 * g, 2 * g + 1):
-            if k:
-                push(esum.at[chunk(k)], back.at[chunk(k)], bs.at[k], br.at[k], ep=k).wait_recv()
-        r = slice(2 * g * cap, (2 * g + 2) * cap)
+            esum[r, :] = value(r).astype(BF16)
+            go(push(esum.at[r], back.at[r], bs.at[k], br.at[k], ep=k))
+
+    def take_far(g):
+        for k in far[g]:
+            push(esum.at[chunk(k)], back.at[chunk(k)], bs.at[k], br.at[k], ep=k).wait_recv()
+        r = span(far[g])
         value = jnp.zeros((length, cols), F32)
         for j in range(hits.shape[0]):
             value += dot(hits[j, :, r], back[r, :]) * weights[:, j:j + 1]
         return value
 
-    far = list(range(eps // 2 - 1, eps // 4 - 1, -1))
-    near = list(range(eps // 4 - 1, 0, -1))
+    scores = scores_ref[...]
+    weights = dot(eye.astype(F32), scores / jnp.sum(scores, axis=0, keepdims=True), ((1,), (1,)), precision=HIGHEST)
+
+    for step in range(heads // per):
+        mix_step(step)
+    go(swap)
     for load in loads[4:7]:
         load.wait()
+    poll(len(agenda) - near_end)
+    poll(2)
     join_states()
-    while len(agenda) > eps:
-        poll(1)
-    feed(0)
-    upward(0)
-    downward(0)
-    poll(len(agenda))
-    for g in near:
+    feed(near, polls=near[-1:])
+    upward(near, polls=(0, 1))
+    downward(near, polls=(1,))
+    give_near()
+    poll(len(agenda) - 1)
+    for g, chunks in enumerate(far):
+        feed(chunks)
+        upward(chunks)
+        if g == 0:
+            poll(1)
+        downward(chunks)
         sums[g][0]()
-    feed(1)
-    upward(1)
-    for g in near:
-        sums[g][1]()
-    downward(1)
-    for g in far:
-        sums[g][0]()
+        if g:
+            sums[g - 1][1]()
+    fold_states()
+    sums[-1][1]()
     finish_mixer()
-    for g in far:
-        sums[g][1]()
     mixsum[0]()
-    for g in near:
-        give_back(g)
-    sums[0][0]()
-    for g in far:
-        give_back(g)
+    for g in range(len(far) - 1):
+        give_far(g)
+    take_near()
+    toksum[0]()
     mixsum[1]()
-    sums[0][1]()
-    value = None
-    for g in near + far:
-        value = combine(g) if value is None else value + combine(g)
+    give_far(len(far) - 1)
+    toksum[1]()
+    value = take_far(0)
+    for g in range(1, len(far)):
+        value += take_far(g)
     total[...] = value
     mixsum[2]()
     mix_out[...] = mixsum[3](slice(0, length)).astype(BF16)
-    give_back(0)
-    moe_out[...] = (total[...] + combine(0)).astype(BF16)
+    toksum[2]()
+    moe_out[...] = (total[...] + toksum[3](slice(0, length))).astype(BF16)
 
     for copy in sent:
         copy.wait_send()
@@ -652,17 +699,19 @@
         pltpu.VMEM((length, cols), BF16), pltpu.VMEM((length, cols), BF16),
         pltpu.VMEM((4, depth, width), BF16), pltpu.VMEM((width, depth), BF16),
         pltpu.VMEM((depth, units), BF16), pltpu.VMEM((depth, units), BF16), pltpu.VMEM((units, depth), BF16),
-        pltpu.VMEM((tps, length, cols), BF16), pltpu.VMEM((length, depth), BF16),
+        pltpu.VMEM((tps, length, cols), BF16), pltpu.VMEM((4, length, width), F32),
         pltpu.VMEM((length, width), F32), pltpu.VMEM((length, width), BF16), pltpu.VMEM((length, width), F32),
         pltpu.VMEM((heads, dim + 16, dim), BF16), pltpu.VMEM((heads, dim + 16, dim), BF16),
-        pltpu.VMEM((heads, dim + 16, dim), BF16), pltpu.VMEM((eps // PAIR, heads, dim + 16, dim), BF16),
+        pltpu.VMEM((heads // 2, dim + 16, dim), BF16), pltpu.VMEM((heads, dim, dim), BF16),
+        pltpu.VMEM((eps // PAIR, heads // 2, dim + 16, dim), BF16),
         pltpu.VMEM((length, width), BF16), pltpu.VMEM((tps, length, cols), BF16), pltpu.VMEM((tps, length, cols), BF16),
         pltpu.VMEM((tps, rows, cols), BF16), pltpu.VMEM((rows, cols), BF16), pltpu.VMEM((top, length, rows), BF16),
-        pltpu.VMEM((rows, depth), BF16), pltpu.VMEM((rows // GROUPS, units), BF16),
+        pltpu.VMEM((rows, depth), BF16), pltpu.VMEM((rows // 2, units), BF16),
         pltpu.VMEM((tps, rows, cols), BF16), pltpu.VMEM((tps, rows, cols), BF16),
+        pltpu.VMEM((tps, rows // 2, cols), BF16), pltpu.VMEM((tps, length, cols), BF16), pltpu.VMEM((tps, length, cols), BF16),
         pltpu.VMEM((rows, cols), BF16), pltpu.VMEM((rows, cols), BF16), pltpu.VMEM((length, cols), F32),
         dma(10), dma(4), dma(4), dma(eps), dma(eps), dma(eps, 4), dma(eps, 4), dma(eps // 2, 6), dma(eps // 2, 6),
-        dma(eps), dma(eps), dma(eps), dma(eps), dma(6), dma(6),
+        dma(eps), dma(eps), dma(eps), dma(eps), dma(6), dma(6), dma(6), dma(6),
     ]
     return pl.pallas_call(
         functools.partial(block_kernel, cap),
@@ -679,7 +728,7 @@
     tokens, cols = mix_rows.shape
     top = route_ids.shape[1]
     cap = tokens * top * 3 // (2 * eps)
-    square = tps == 4 and eps >= 4 and eps & (eps - 1) == 0
+    square = tps == 4 and dec.shape[0] % 2 == 0 and eps >= 4 and eps & (eps - 1) == 0
     aligned = cap % 32 == 0 and cols % 128 == 0 and tokens % (2 * BLOCK) == 0 and w_gate.shape[2] % 128 == 0
     return square and aligned and w_gate.shape[0] == 1
 

time: 86.2 us -> 80 us (0.928); the launches traced: 85.7 us -> 78.6 us
  Pallas kernels: 81.7 us -> 74.6 us
    pallas_call x1, Pallas kernels: 81.7 us -> 74.6 us  [whole_block(): pl.pallas_call(functools.partial(block_kernel, cap), in_specs=[ANY, VMEM,...]
where the time goes in v3:
time: 80 us; the launch traced here: 78.6 us
  Pallas kernels  74.6 us (93%)
  local copies, waits for them, and re-layouts  3.34 us (4%)
    pallas_call x1, Pallas kernels, whole_block(): pl.pallas_call(functools.partial(block_kernel, cap), in_specs=[ANY, VMEM,...  74.6 us
    unnamed x2, local copies, waits for them, and re-layouts  3.34 us

profile of v3, /device:TPU:0, one launch (start us, length us, event | category | flops | bytes accessed | tf_op | source)
XLA Modules:
  0.0 78.6 jit_solution(3028376342764920234)
XLA Ops:
  0.6 74.6 %shard_map.176 = (bf16[256,512]{1,0:T(8,128)(2,1)}, bf16[256,512]{1,0:T(8,128)(2,1)}) custom-call(bf16[256,512]{1,0:T(8,128)(2,1)} %mix_hbm.1, bf16[16,128]{1,0:T(8,128)(2,1)} %bitcast.6, bf16[2048,512]{1,0:T(8,128)(2,1)} %wq_hbm.1, bf16[2048,512]{1,0:T(8,128)(2,1)} %wf_hbm.1, bf16[2048,512]{1,0:T(8,128)(2,1)} %wi_hbm.1, bf16[2048,512]{1,0:T(8,128)(2,1)} %wo_hbm.1, ...), custom_call_target="tpu_custom_call" | custom-call | tf_op jit(solution)/shard_map/pallas_call | solution.py:716
  75.3 1.7 %copy.21 = bf16[256,512]{1,0:T(8,128)(2,1)} copy(bf16[256,512]{1,0:T(8,128)(2,1)} %get-tuple-element.4) | data formatting | bytes 524288
  76.9 1.7 %copy.22 = bf16[256,512]{1,0:T(8,128)(2,1)} copy(bf16[256,512]{1,0:T(8,128)(2,1)} %get-tuple-element.5) | data formatting | bytes 524288

commit v4 on v3

--- a/solution.py
+++ b/solution.py
@@ -267,12 +267,12 @@
     return place
 
 
-def block_kernel(cap, mix_hbm, mgain_ref, wq_hbm, wf_hbm, wi_hbm, wo_hbm, gap_ref, dec_ref, hgain_ref, wm_hbm,
-                 moe_hbm, egain_ref, ids_ref, scores_ref, wg_hbm, wu_hbm, wd_hbm,
-                 mix_out, moe_out,
+def block_kernel(cap, mix_hbm, mgain_hbm, wq_hbm, wf_hbm, wi_hbm, wo_hbm, gap_hbm, dec_hbm, hgain_hbm, wm_hbm,
+                 moe_hbm, egain_hbm, ids_hbm, scores_hbm, wg_hbm, wu_hbm, wd_hbm,
+                 mix_out, moe_out, mgain_ref, gap_ref, dec_ref, hgain_ref, egain_ref, ids_ref, scores_ref,
                  mix_ref, moe_ref, wmix, wm, wg, wu, wd, xall, acc, lo, qd, og, st, pst, cst, fst, states, gated, mixed, mixin,
                  gath, slots, hits, enormed, hidden, psend, precv, nback, tok, tokin, esum, back, total,
-                 wsem, xs, xr, zs, zr, gs, gr, ps, pr, bs, br, ss, sr, ms, mr, ts, tr):
+                 wsem, out_sem, xr, zr, gr, pr, br, sr, mr, tr):
     eps, tps = lax.axis_size("ep"), lax.axis_size("tp")
     me, mt = lax.axis_index("ep"), lax.axis_index("tp")
     length, cols = mix_ref.shape
@@ -283,9 +283,9 @@
     ep_peer = [flip(me, k) for k in range(eps)]
     tp_peer = [flip(mt, r) for r in range(tps)]
 
-    def push(src, dst, send, recv, ep=None, tp=None):
+    def push(src, dst, recv, ep=None, tp=None):
         where = {"ep": ep_peer[ep]} if tp is None else {"tp": tp_peer[tp]}
-        return pltpu.make_async_remote_copy(src_ref=src, dst_ref=dst, send_sem=send, recv_sem=recv,
+        return pltpu.make_async_remote_copy(src_ref=src, dst_ref=dst, send_sem=out_sem.at[0], recv_sem=recv,
                                             device_id=where, device_id_type=MESH)
 
     sent = []
@@ -294,27 +294,29 @@
         copy.start()
         sent.append(copy)
 
-    loads = [pltpu.make_async_copy(s, wmix.at[i], wsem.at[i]) for i, s in enumerate((wq_hbm, wf_hbm, wi_hbm, wo_hbm))]
-    loads += [pltpu.make_async_copy(wg_hbm.at[0], wg, wsem.at[4]), pltpu.make_async_copy(wu_hbm.at[0], wu, wsem.at[5]),
-              pltpu.make_async_copy(wd_hbm.at[0], wd, wsem.at[6]), pltpu.make_async_copy(wm_hbm, wm, wsem.at[7])]
-    rowload = [pltpu.make_async_copy(mix_hbm, mix_ref, wsem.at[8]), pltpu.make_async_copy(moe_hbm, moe_ref, wsem.at[9])]
-
+    loads = [pltpu.make_async_copy(s, wmix.at[i], wsem.at[0]) for i, s in enumerate((wq_hbm, wf_hbm, wi_hbm, wo_hbm))]
+    loads += [pltpu.make_async_copy(wg_hbm.at[0], wg, wsem.at[1]), pltpu.make_async_copy(wu_hbm.at[0], wu, wsem.at[2]),
+              pltpu.make_async_copy(wd_hbm.at[0], wd, wsem.at[3]), pltpu.make_async_copy(wm_hbm, wm, wsem.at[4])]
     barrier = pltpu.get_barrier_semaphore()
     for k in range(1, eps):
         pl.semaphore_signal(barrier, inc=1, device_id={"ep": ep_peer[k]}, device_id_type=MESH)
     for r in range(1, tps):
         pl.semaphore_signal(barrier, inc=1, device_id={"tp": tp_peer[r]}, device_id_type=MESH)
+    small = [(mix_hbm, mix_ref), (ids_hbm, ids_ref), (moe_hbm, moe_ref), (mgain_hbm, mgain_ref), (gap_hbm, gap_ref),
+             (dec_hbm, dec_ref), (hgain_hbm, hgain_ref), (egain_hbm, egain_ref), (scores_hbm, scores_ref)]
+    rowload = [pltpu.make_async_copy(src, dst, wsem.at[5 + i]) for i, (src, dst) in enumerate(small)]
     for load in rowload + loads:
         load.start()
     rowload[0].wait()
     pl.semaphore_wait(barrier, eps + tps - 2)
 
     half = length // 2
-    go(push(mix_ref, xall.at[mt], xs.at[0], xr.at[0], tp=1))
-    go(push(mix_ref, xall.at[mt], xs.at[1], xr.at[1], tp=2))
+    go(push(mix_ref, xall.at[mt], xr.at[0], tp=1))
+    go(push(mix_ref, xall.at[mt], xr.at[1], tp=2))
 
     experts = eps
     names = iota((length, experts), 1)
+    rowload[1].wait()
     eye = iota((length, length), 0) == iota((length, length), 1)
     ids = dot(eye.astype(BF16), ids_ref[...].astype(F32).astype(BF16), ((1,), (1,))).astype(jnp.int32)
     picks = [ids[:, j:j + 1] == names for j in range(ids.shape[1])]
@@ -322,7 +324,7 @@
     before = (iota((length, length), 0) > iota((length, length), 1)).astype(BF16)
     rank = dot(before, chosen.astype(BF16)).astype(jnp.int32)
     spot = rank + jnp.bitwise_xor(names, me) * cap
-    rowload[1].wait()
+    rowload[2].wait()
     both = None
     for j, pick in enumerate(picks):
         at = jnp.sum(jnp.where(pick, spot, 0), axis=1, keepdims=True)
@@ -334,7 +336,7 @@
     gath[mt, 0:cap, :] = made[0:cap]
     for k in range(1, eps):
         r = slice(k * cap, (k + 1) * cap)
-        go(push(slots.at[r], gath.at[mt, r], zs.at[k], zr.at[k], ep=k))
+        go(push(slots.at[r], gath.at[mt, r], zr.at[k], ep=k))
 
     def rowsof(k, part=None):
         if part is None:
@@ -343,48 +345,49 @@
 
     def spread(k):
         if k:
-            push(slots.at[rowsof(k)], gath.at[mt, rowsof(k)], zs.at[k], zr.at[k], ep=k).wait_recv()
+            push(slots.at[rowsof(k)], gath.at[mt, rowsof(k)], zr.at[k], ep=k).wait_recv()
         for n, r in enumerate((1, 2)):
             ref = gath.at[mt, rowsof(k)]
-            go(push(ref, ref, gs.at[k, n], gr.at[k, n], tp=r))
+            go(push(ref, ref, gr.at[k, n], tp=r))
 
     def relay(k):
         for n, (source, target) in enumerate(((1, 2), (2, 1))):
             whole = gath.at[tp_peer[source], rowsof(k)]
-            push(whole, whole, gs.at[k, n], gr.at[k, n], tp=source).wait_recv()
+            push(whole, whole, gr.at[k, n], tp=source).wait_recv()
             ref = gath.at[tp_peer[source], rowsof(k, n)]
-            go(push(ref, ref, gs.at[k, 2 + n], gr.at[k, 2 + n], tp=target))
+            go(push(ref, ref, gr.at[k, 2], tp=target))
 
     def complete(k):
-        for n, via in enumerate((2, 1)):
-            ref = gath.at[tp_peer[3], rowsof(k, n)]
-            push(ref, ref, gs.at[k, 2 + n], gr.at[k, 2 + n], tp=via).wait_recv()
+        ref = gath.at[tp_peer[3], rowsof(k)]
+        push(ref, ref, gr.at[k, 2], tp=1).wait_recv()
 
     def relay_mix():
         for n, (source, target) in enumerate(((1, 2), (2, 1))):
             whole = xall.at[tp_peer[source]]
-            push(whole, whole, xs.at[n], xr.at[n], tp=source).wait_recv()
+            push(whole, whole, xr.at[n], tp=source).wait_recv()
             ref = xall.at[tp_peer[source], pl.ds(n * half, half)]
-            go(push(ref, ref, xs.at[2 + n], xr.at[2 + n], tp=target))
+            go(push(ref, ref, xr.at[2], tp=target))
 
     def complete_mix():
-        for n, via in enumerate((2, 1)):
-            ref = xall.at[tp_peer[3], pl.ds(n * half, half)]
-            push(ref, ref, xs.at[2 + n], xr.at[2 + n], tp=via).wait_recv()
+        ref = xall.at[tp_peer[3]]
+        push(ref, ref, xr.at[2], tp=1).wait_recv()
 
     S, R = (lambda k: functools.partial(spread, k)), (lambda k: functools.partial(relay, k))
-    agenda = []
-    for k in range(1, eps):
-        agenda += [S(k + 2), R(k)] if k + 2 < eps else [R(k)]
-    spot = 2 * (eps // 2 - 1) - 1
-    if eps // 2 + 1 < eps:
-        agenda[spot - 1:spot + 1] = agenda[spot - 1:spot + 1][::-1]
-    near_end = len(agenda) - spot if eps // 2 + 1 < eps else 0
+    agenda, ahead = [], eps // 2
+    for k in range(1, ahead):
+        agenda += [S(k + 2), R(k)] if k + 2 < ahead else [R(k)]
+    far_start = len(agenda)
+    spreads, relays = [S(k) for k in range(max(ahead, 3), eps)], [R(k) for k in range(ahead, eps)]
+    agenda += spreads[:3]
+    agenda += relays[:2] + spreads[3:] + relays[2:]
+    far_end = len(agenda) - far_start
 
     def poll(count=1):
         for _ in range(min(count, len(agenda))):
             agenda.pop(0)()
 
+    for load in rowload[3:]:
+        load.wait()
     mgain, egain = mgain_ref[...].astype(F32), egain_ref[...].astype(F32)
     lanes = mgain.shape[1]
     per_shard = cols // lanes
@@ -405,8 +408,7 @@
             acc[i] = part if first else acc[i] + part
 
     S(0)()
-    for load in loads[:4]:
-        load.wait()
+    pltpu.make_async_copy(wmix, wmix, wsem.at[0]).wait()
     project(0, mix_ref, True)
     relay_mix()
     S(1)()
@@ -461,17 +463,18 @@
                 base = last
             st[h, 0:dim, :] = state.astype(BF16)
             st[h, dim:, :] = jnp.broadcast_to(jnp.exp(base), (st.shape[1] - dim, dim)).astype(BF16)
-            poll(1)
+            if h:
+                poll(1)
 
     odd = lax.rem(me, PAIR)
     pair = lax.div(me, PAIR)
-    swap = push(st, pst, ss.at[1], sr.at[0], ep=1)
+    swap = push(st, pst, sr.at[0], ep=1)
     own_half = pl.ds(odd * (heads // 2), heads // 2)
     other_half = pl.ds((1 - odd) * (heads // 2), heads // 2)
-    trade = push(fst.at[own_half], fst.at[own_half], ss.at[0], sr.at[eps - 1], ep=1)
+    trade = push(fst.at[own_half], fst.at[own_half], sr.at[1 + eps // PAIR], ep=1)
 
     def joined_copy(k):
-        return push(cst, states.at[pair], ss.at[k], sr.at[1 + pair], ep=k)
+        return push(cst, states.at[pair], sr.at[1 + pair], ep=k)
 
     def parts_of(ref, h):
         return ref[h, 0:dim, :].astype(F32), ref[h, dim:dim + 16, :].astype(F32)[0:1]
@@ -491,7 +494,7 @@
     def fold_states():
         @pl.loop(0, pair)
         def _(hop):
-            pltpu.make_async_remote_copy(src_ref=cst, dst_ref=states.at[hop], send_sem=ss.at[0], recv_sem=sr.at[1 + hop],
+            pltpu.make_async_remote_copy(src_ref=cst, dst_ref=states.at[hop], send_sem=out_sem.at[0], recv_sem=sr.at[1 + hop],
                                          device_id={"ep": hop * PAIR + odd}, device_id_type=MESH).wait_recv()
 
         for i in range(heads // 2):
@@ -504,7 +507,7 @@
         go(trade)
 
     def finish_mixer():
-        push(fst.at[other_half], fst.at[other_half], ss.at[0], sr.at[eps - 1], ep=1).wait_recv()
+        push(fst.at[other_half], fst.at[other_half], sr.at[1 + eps // PAIR], ep=1).wait_recv()
         for h in range(heads):
             c = slice(h * dim, (h + 1) * dim)
             state = fst[h].astype(F32)
@@ -519,10 +522,8 @@
             mixed[r] = dot(gated[...], block).astype(BF16)
 
     tile = 256 if units % 256 == 0 else units
-    def feed(chunks, polls=()):
+    def feed(chunks):
         for k in chunks:
-            if k in polls:
-                poll(1)
             complete(k)
             r = chunk(k)
             squares = jnp.zeros((cap, 1), F32)
@@ -561,12 +562,13 @@
             if t in polls:
                 poll(1)
 
-    def summing(src, dst, a, b, send, recv):
+    def summing(src, dst, a, b, recv):
         def part(n, index, target, r, tp):
-            return push(src.at[index, r], dst.at[target, r], send.at[n], recv.at[n], tp=tp)
-
-        first = [part(0, 3, 3, a, 1), part(1, 3, 3, b, 2), part(2, 1, 1, a, 1), part(3, 2, 2, b, 2)]
-        second = [part(4, 2, 2, a, 2), part(5, 1, 1, b, 1)]
+            return push(src.at[index, r], dst.at[target, r], recv.at[n], tp=tp)
+
+        first = [part(0, 3, 3, a, 1), part(1, 3, 3, b, 2), part(2, 1, 1, a, 1), part(2, 2, 2, b, 2)]
+        second = [part(2, 2, 2, a, 2), part(2, 1, 1, b, 1)]
+        landed = dst.at[pl.ds(1, 2), slice(a.start, b.stop)]
 
         def start():
             for copy in first:
@@ -581,8 +583,7 @@
                 go(copy)
 
         def finish():
-            for copy in first[2:] + second:
-                copy.wait_recv()
+            push(landed, landed, recv.at[2], tp=1).wait_recv()
 
         def value(r):
             return src[0, r, :].astype(F32) + dst[1, r, :].astype(F32) + dst[2, r, :].astype(F32)
@@ -592,12 +593,12 @@
     near = list(range(eps // 2))
     far = [[k, k + 1] for k in range(eps // 2, eps, 2)]
     nrows = len(near) * cap
-    sums = [summing(psend, precv, chunk(a), chunk(b), ps.at[g], pr.at[g]) for g, (a, b) in enumerate(far)]
-    mixsum = summing(mixed, mixin, slice(0, half), slice(half, length), ms, mr)
-    toksum = summing(tok, tokin, slice(0, half), slice(half, length), ts, tr)
+    sums = [summing(psend, precv, chunk(a), chunk(b), pr.at[g]) for g, (a, b) in enumerate(far)]
+    mixsum = summing(mixed, mixin, slice(0, half), slice(half, length), mr)
+    toksum = summing(tok, tokin, slice(0, half), slice(half, length), tr)
 
     def near_copy(k):
-        return push(psend.at[:, chunk(k)], nback.at[:, chunk(k)], bs.at[k], br.at[k], ep=k)
+        return push(psend.at[:, chunk(k)], nback.at[:, chunk(k)], br.at[0], ep=k)
 
     def give_near():
         for k in near[1:]:
@@ -605,8 +606,8 @@
         nback[:, chunk(0), :] = psend[:, chunk(0), :]
 
     def take_near():
-        for k in near[1:]:
-            near_copy(k).wait_recv()
+        landed = nback.at[:, span(near[1:])]
+        push(landed, landed, br.at[0], ep=1).wait_recv()
         for t in (3, 1, 2, 0):
             value = jnp.zeros((length, cols), F32)
             for j in range(hits.shape[0]):
@@ -619,12 +620,11 @@
         for k in far[g]:
             r = chunk(k)
             esum[r, :] = value(r).astype(BF16)
-            go(push(esum.at[r], back.at[r], bs.at[k], br.at[k], ep=k))
+            go(push(esum.at[r], back.at[r], br.at[1 + g], ep=k))
 
     def take_far(g):
-        for k in far[g]:
-            push(esum.at[chunk(k)], back.at[chunk(k)], bs.at[k], br.at[k], ep=k).wait_recv()
         r = span(far[g])
+        push(back.at[r], back.at[r], br.at[1 + g], ep=1).wait_recv()
         value = jnp.zeros((length, cols), F32)
         for j in range(hits.shape[0]):
             value += dot(hits[j, :, r], back[r, :]) * weights[:, j:j + 1]
@@ -638,20 +638,20 @@
     go(swap)
     for load in loads[4:7]:
         load.wait()
-    poll(len(agenda) - near_end)
+    poll(len(agenda) - far_end)
     poll(2)
     join_states()
-    feed(near, polls=near[-1:])
-    upward(near, polls=(0, 1))
-    downward(near, polls=(1,))
+    feed(near)
+    upward(near, polls=(1,))
+    downward(near, polls=(1, 2))
     give_near()
     poll(len(agenda) - 1)
     for g, chunks in enumerate(far):
         feed(chunks)
-        upward(chunks)
+        upward(chunks, polls=(1,))
+        downward(chunks)
         if g == 0:
-            poll(1)
-        downward(chunks)
+            poll(len(agenda))
         sums[g][0]()
         if g:
             sums[g - 1][1]()
@@ -683,6 +683,14 @@
             joined_copy(k).wait_send()
 
 
+def place_kernel(a_ref, b_ref, a_out, b_out, sem):
+    copies = [pltpu.make_async_copy(a_ref, a_out, sem.at[0]), pltpu.make_async_copy(b_ref, b_out, sem.at[1])]
+    for copy in copies:
+        copy.start()
+    for copy in copies:
+        copy.wait()
+
+
 def whole_block(mix_rows, mix_gain, wq, wf, wi, wo, gap, dec, hgain, wm, moe_rows, moe_gain, ids, scores, wg, wu, wd):
     eps, tps = lax.axis_size("ep"), lax.axis_size("tp")
     length, cols = mix_rows.shape
@@ -696,6 +704,9 @@
     dma = lambda *s: pltpu.SemaphoreType.DMA(s)
     out = jax.ShapeDtypeStruct((length, cols), BF16)
     scratch = [
+        pltpu.VMEM((depth // 128, 128), BF16), pltpu.VMEM((1, width), F32), pltpu.VMEM(dec.shape, F32),
+        pltpu.VMEM((1, dim), BF16), pltpu.VMEM((depth // 128, 128), BF16),
+        pltpu.VMEM((top, length), jnp.int32), pltpu.VMEM((top, length), F32),
         pltpu.VMEM((length, cols), BF16), pltpu.VMEM((length, cols), BF16),
         pltpu.VMEM((4, depth, width), BF16), pltpu.VMEM((width, depth), BF16),
         pltpu.VMEM((depth, units), BF16), pltpu.VMEM((depth, units), BF16), pltpu.VMEM((units, depth), BF16),
@@ -710,18 +721,26 @@
         pltpu.VMEM((tps, rows, cols), BF16), pltpu.VMEM((tps, rows, cols), BF16),
         pltpu.VMEM((tps, rows // 2, cols), BF16), pltpu.VMEM((tps, length, cols), BF16), pltpu.VMEM((tps, length, cols), BF16),
         pltpu.VMEM((rows, cols), BF16), pltpu.VMEM((rows, cols), BF16), pltpu.VMEM((length, cols), F32),
-        dma(10), dma(4), dma(4), dma(eps), dma(eps), dma(eps, 4), dma(eps, 4), dma(eps // 2, 6), dma(eps // 2, 6),
-        dma(eps), dma(eps), dma(eps), dma(eps), dma(6), dma(6), dma(6), dma(6),
+        dma(14), dma(1), dma(3), dma(eps), dma(eps, 3), dma(eps // 4, 3), dma(1 + eps // 4),
+        dma(2 + eps // PAIR), dma(3), dma(3),
     ]
-    return pl.pallas_call(
+    results = pl.pallas_call(
         functools.partial(block_kernel, cap),
-        in_specs=[ANY, VMEM, ANY, ANY, ANY, ANY, VMEM, VMEM, VMEM, ANY, ANY, VMEM, VMEM, VMEM, ANY, ANY, ANY],
+        in_specs=[pl.BlockSpec(memory_space=pltpu.HBM)] * 17,
         out_specs=[VMEM, VMEM],
-        out_shape=[out, out],
+        out_shape=[pltpu.VMEM((length, cols), BF16)] * 2,
         scratch_shapes=scratch,
         compiler_params=pltpu.CompilerParams(vmem_limit_bytes=LIMIT, collective_id=0, has_side_effects=True),
     )(mix_rows, mix_gain.reshape(-1, 128), wq, wf, wi, wo, gap.reshape(1, -1), dec, hgain.reshape(1, -1), wm,
       moe_rows, moe_gain.reshape(-1, 128), ids.T, scores.T, wg, wu, wd)
+    return pl.pallas_call(
+        place_kernel,
+        in_specs=[VMEM, VMEM],
+        out_specs=[ANY, ANY],
+        out_shape=[out, out],
+        scratch_shapes=[dma(2)],
+        compiler_params=pltpu.CompilerParams(vmem_limit_bytes=1024 * 1024),
+    )(*results)
 
 
 def fits(eps, tps, mix_rows, dec, route_ids, w_gate):

time: 80 us -> 74.6 us (0.932); the launches traced: 78.6 us -> 74.4 us
  local copies, waits for them, and re-layouts: 3.34 us -> 0 us
  Pallas kernels: 74.6 us -> 73.6 us
    unnamed x2 -> x0, local copies, waits for them, and re-layouts: 3.34 us -> none
    pallas_call x1 -> x2, Pallas kernels: 74.6 us -> 73.6 us  [the longest x1 72.8 us: whole_block(): pl.pallas_call(functools.partial(block_kernel, cap), in_specs=[pl.BlockSp...]
where the time goes in v4:
time: 74.6 us; the launch traced here: 74.4 us
  Pallas kernels  73.6 us (99%)
  between operations  0.81 us (1%)
    pallas_call x1, Pallas kernels, whole_block(): pl.pallas_call(functools.partial(block_kernel, cap), in_specs=[pl.BlockSp...  72.8 us

profile of v4, /device:TPU:0, one launch (start us, length us, event | category | flops | bytes accessed | tf_op | source)
XLA Modules:
  0.0 74.4 jit_solution(13733045588417892250)
XLA Ops:
  0.6 72.8 %shard_map.176 = (bf16[256,512]{1,0:T(8,128)(2,1)S(1)}, bf16[256,512]{1,0:T(8,128)(2,1)S(1)}) custom-call(bf16[256,512]{1,0:T(8,128)(2,1)} %mix_hbm.1, bf16[16,128]{1,0:T(8,128)(2,1)} %bitcast.6, bf16[2048,512]{1,0:T(8,128)(2,1)} %wq_hbm.1, bf16[2048,512]{1,0:T(8,128)(2,1)} %wf_hbm.1, bf16[2048,512]{1,0:T(8,128)(2,1)} %wi_hbm.1, bf16[2048,512]{1,0:T(8,128)(2,1)} %wo_hbm.1, ...), custom_call_target="tpu_custom_call" | custom-call | tf_op jit(solution)/shard_map/pallas_call | solution.py:727
  73.4 0.8 %shard_map.177 = (bf16[256,512]{1,0:T(8,128)(2,1)}, bf16[256,512]{1,0:T(8,128)(2,1)}) custom-call(bf16[256,512]{1,0:T(8,128)(2,1)S(1)} %get-tuple-element.4.a_ref, bf16[256,512]{1,0:T(8,128)(2,1)S(1)} %get-tuple-element.5.b_ref), custom_call_target="tpu_custom_call" | custom-call | tf_op jit(solution)/shard_map/pallas_call | solution.py:736

commit v5 on v4

--- a/solution.py
+++ b/solution.py
@@ -410,8 +410,8 @@
     S(0)()
     pltpu.make_async_copy(wmix, wmix, wsem.at[0]).wait()
     project(0, mix_ref, True)
+    S(1)()
     relay_mix()
-    S(1)()
     project(1, xall.at[tp_peer[1]], False)
     R(0)()
     S(2)()
@@ -570,8 +570,8 @@
         second = [part(2, 2, 2, a, 2), part(2, 1, 1, b, 1)]
         landed = dst.at[pl.ds(1, 2), slice(a.start, b.stop)]
 
-        def start():
-            for copy in first:
+        def start(pieces=slice(0, 4)):
+            for copy in first[pieces]:
                 go(copy)
 
         def merge():
@@ -646,24 +646,25 @@
     downward(near, polls=(1, 2))
     give_near()
     poll(len(agenda) - 1)
+    fold_states()
+    finish_mixer()
+    mixsum[0](slice(0, 2))
     for g, chunks in enumerate(far):
         feed(chunks)
         upward(chunks, polls=(1,))
+        if g:
+            sums[g - 1][1]()
         downward(chunks)
         if g == 0:
             poll(len(agenda))
         sums[g][0]()
-        if g:
-            sums[g - 1][1]()
-    fold_states()
-    sums[-1][1]()
-    finish_mixer()
-    mixsum[0]()
+    mixsum[0](slice(2, 4))
     for g in range(len(far) - 1):
         give_far(g)
+    sums[-1][1]()
+    mixsum[1]()
     take_near()
     toksum[0]()
-    mixsum[1]()
     give_far(len(far) - 1)
     toksum[1]()
     value = take_far(0)

time: 74.6 us -> 74 us (level)
  no operation moved by 1% of the time
where the time goes in v5:
time: 74 us; the launch traced here: 73.8 us
  Pallas kernels  73 us (99%)
  between operations  0.81 us (1%)
    pallas_call x1, Pallas kernels, whole_block(): pl.pallas_call(functools.partial(block_kernel, cap), in_specs=[pl.BlockSp...  72.2 us

profile of v5, /device:TPU:0, one launch (start us, length us, event | category | flops | bytes accessed | tf_op | source)
XLA Modules:
  0.0 73.8 jit_solution(9508121638725686011)
XLA Ops:
  0.6 72.2 %shard_map.176 = (bf16[256,512]{1,0:T(8,128)(2,1)S(1)}, bf16[256,512]{1,0:T(8,128)(2,1)S(1)}) custom-call(bf16[256,512]{1,0:T(8,128)(2,1)} %mix_hbm.1, bf16[16,128]{1,0:T(8,128)(2,1)} %bitcast.6, bf16[2048,512]{1,0:T(8,128)(2,1)} %wq_hbm.1, bf16[2048,512]{1,0:T(8,128)(2,1)} %wf_hbm.1, bf16[2048,512]{1,0:T(8,128)(2,1)} %wi_hbm.1, bf16[2048,512]{1,0:T(8,128)(2,1)} %wo_hbm.1, ...), custom_call_target="tpu_custom_call" | custom-call | tf_op jit(solution)/shard_map/pallas_call | solution.py:728
  72.8 0.8 %shard_map.177 = (bf16[256,512]{1,0:T(8,128)(2,1)}, bf16[256,512]{1,0:T(8,128)(2,1)}) custom-call(bf16[256,512]{1,0:T(8,128)(2,1)S(1)} %get-tuple-element.4.a_ref, bf16[256,512]{1,0:T(8,128)(2,1)S(1)} %get-tuple-element.5.b_ref), custom_call_target="tpu_custom_call" | custom-call | tf_op jit(solution)/shard_map/pallas_call | solution.py:737

commit v6 on v5

--- a/solution.py
+++ b/solution.py
@@ -272,7 +272,7 @@
                  mix_out, moe_out, mgain_ref, gap_ref, dec_ref, hgain_ref, egain_ref, ids_ref, scores_ref,
                  mix_ref, moe_ref, wmix, wm, wg, wu, wd, xall, acc, lo, qd, og, st, pst, cst, fst, states, gated, mixed, mixin,
                  gath, slots, hits, enormed, hidden, psend, precv, nback, tok, tokin, esum, back, total,
-                 wsem, out_sem, xr, zr, gr, pr, br, sr, mr, tr):
+                 wsem, free_sem, out_sem, xr, zr, gr, pr, br, sr, mr, tr):
     eps, tps = lax.axis_size("ep"), lax.axis_size("tp")
     me, mt = lax.axis_index("ep"), lax.axis_index("tp")
     length, cols = mix_ref.shape
@@ -298,17 +298,34 @@
     loads += [pltpu.make_async_copy(wg_hbm.at[0], wg, wsem.at[1]), pltpu.make_async_copy(wu_hbm.at[0], wu, wsem.at[2]),
               pltpu.make_async_copy(wd_hbm.at[0], wd, wsem.at[3]), pltpu.make_async_copy(wm_hbm, wm, wsem.at[4])]
     barrier = pltpu.get_barrier_semaphore()
-    for k in range(1, eps):
-        pl.semaphore_signal(barrier, inc=1, device_id={"ep": ep_peer[k]}, device_id_type=MESH)
-    for r in range(1, tps):
+    leader = tps - 1
+    leads = jnp.logical_and(lax.rem(me, PAIR) == 0, mt == leader)
+    for j in range(eps // PAIR):
+        @pl.when(jnp.logical_or(me != j * PAIR, mt != leader))
+        def _():
+            pl.semaphore_signal(barrier, inc=1, device_id={"ep": j * PAIR, "tp": leader}, device_id_type=MESH)
+    for r in (1, 2):
         pl.semaphore_signal(barrier, inc=1, device_id={"tp": tp_peer[r]}, device_id_type=MESH)
+    pl.semaphore_signal(barrier, inc=1, device_id={"ep": ep_peer[1]}, device_id_type=MESH)
     small = [(mix_hbm, mix_ref), (ids_hbm, ids_ref), (moe_hbm, moe_ref), (mgain_hbm, mgain_ref), (gap_hbm, gap_ref),
              (dec_hbm, dec_ref), (hgain_hbm, hgain_ref), (egain_hbm, egain_ref), (scores_hbm, scores_ref)]
     rowload = [pltpu.make_async_copy(src, dst, wsem.at[5 + i]) for i, (src, dst) in enumerate(small)]
     for load in rowload + loads:
         load.start()
     rowload[0].wait()
-    pl.semaphore_wait(barrier, eps + tps - 2)
+
+    @pl.when(leads)
+    def _():
+        pl.semaphore_wait(barrier, 3 + eps * tps - 1)
+        for c in range(PAIR):
+            for t in range(tps):
+                if c or t != leader:
+                    pl.semaphore_signal(free_sem, inc=1, device_id={"ep": me + c, "tp": t}, device_id_type=MESH)
+
+    @pl.when(jnp.logical_not(leads))
+    def _():
+        pl.semaphore_wait(barrier, 3)
+
 
     half = length // 2
     go(push(mix_ref, xall.at[mt], xr.at[0], tp=1))
@@ -334,7 +351,7 @@
     made = dot(both.astype(BF16), moe_ref[...], ((0,), (0,))).astype(BF16)
     slots[...] = made
     gath[mt, 0:cap, :] = made[0:cap]
-    for k in range(1, eps):
+    def send_slots(k):
         r = slice(k * cap, (k + 1) * cap)
         go(push(slots.at[r], gath.at[mt, r], zr.at[k], ep=k))
 
@@ -407,7 +424,15 @@
             part = dot(v, wmix[i, w, :])
             acc[i] = part if first else acc[i] + part
 
+    send_slots(1)
     S(0)()
+
+    @pl.when(jnp.logical_not(leads))
+    def _():
+        pl.semaphore_wait(free_sem, 1)
+
+    for k in range(2, eps):
+        send_slots(k)
     pltpu.make_async_copy(wmix, wmix, wsem.at[0]).wait()
     project(0, mix_ref, True)
     S(1)()
@@ -722,7 +747,7 @@
         pltpu.VMEM((tps, rows, cols), BF16), pltpu.VMEM((tps, rows, cols), BF16),
         pltpu.VMEM((tps, rows // 2, cols), BF16), pltpu.VMEM((tps, length, cols), BF16), pltpu.VMEM((tps, length, cols), BF16),
         pltpu.VMEM((rows, cols), BF16), pltpu.VMEM((rows, cols), BF16), pltpu.VMEM((length, cols), F32),
-        dma(14), dma(1), dma(3), dma(eps), dma(eps, 3), dma(eps // 4, 3), dma(1 + eps // 4),
+        dma(14), pltpu.SemaphoreType.REGULAR, dma(1), dma(3), dma(eps), dma(eps, 3), dma(eps // 4, 3), dma(1 + eps // 4),
         dma(2 + eps // PAIR), dma(3), dma(3),
     ]
     results = pl.pallas_call(

time: 74 us -> 71.7 us (0.969)
  Pallas kernels: 73 us -> 70.8 us
    pallas_call x1, Pallas kernels: 72.2 us -> 70 us  [whole_block(): pl.pallas_call(functools.partial(block_kernel, cap), in_specs=[pl.BlockSp...]
where the time goes in v6:
time: 71.7 us; the launch traced here: 71.6 us
  Pallas kernels  70.8 us (99%)
  between operations  0.81 us (1%)
    pallas_call x1, Pallas kernels, whole_block(): pl.pallas_call(functools.partial(block_kernel, cap), in_specs=[pl.BlockSp...  70 us

profile of v6, /device:TPU:0, one launch (start us, length us, event | category | flops | bytes accessed | tf_op | source)
XLA Modules:
  0.0 71.6 jit_solution(12561030866488609708)
XLA Ops:
  0.6 70.0 %shard_map.176 = (bf16[256,512]{1,0:T(8,128)(2,1)S(1)}, bf16[256,512]{1,0:T(8,128)(2,1)S(1)}) custom-call(bf16[256,512]{1,0:T(8,128)(2,1)} %mix_hbm.1, bf16[16,128]{1,0:T(8,128)(2,1)} %bitcast.6, bf16[2048,512]{1,0:T(8,128)(2,1)} %wq_hbm.1, bf16[2048,512]{1,0:T(8,128)(2,1)} %wf_hbm.1, bf16[2048,512]{1,0:T(8,128)(2,1)} %wi_hbm.1, bf16[2048,512]{1,0:T(8,128)(2,1)} %wo_hbm.1, ...), custom_call_target="tpu_custom_call" | custom-call | tf_op jit(solution)/shard_map/pallas_call | solution.py:753
  70.6 0.8 %shard_map.177 = (bf16[256,512]{1,0:T(8,128)(2,1)}, bf16[256,512]{1,0:T(8,128)(2,1)}) custom-call(bf16[256,512]{1,0:T(8,128)(2,1)S(1)} %get-tuple-element.4.a_ref, bf16[256,512]{1,0:T(8,128)(2,1)S(1)} %get-tuple-element.5.b_ref), custom_call_target="tpu_custom_call" | custom-call | tf_op jit(solution)/shard_map/pallas_call | solution.py:762

commit v7 on v6

--- a/solution.py
+++ b/solution.py
@@ -569,13 +569,14 @@
     def span(chunks):
         return slice(chunks[0] * cap, (chunks[-1] + 1) * cap)
 
-    def upward(chunks, polls=()):
+    def upward(chunks, polls=(), skip=0):
         r = span(chunks)
+        rows_to = slice(skip * cap, (skip + len(chunks)) * cap)
         for u in range(units // tile):
             c = slice(u * tile, (u + 1) * tile)
             gate = dot(enormed[r, :], wg[:, c])
             up = dot(enormed[r, :], wu[:, c])
-            hidden[0:len(chunks) * cap, c] = (gate * sigmoid(gate) * up).astype(BF16)
+            hidden[rows_to, c] = (gate * sigmoid(gate) * up).astype(BF16)
             if u in polls:
                 poll(1)
 
@@ -666,8 +667,10 @@
     poll(len(agenda) - far_end)
     poll(2)
     join_states()
-    feed(near)
-    upward(near, polls=(1,))
+    feed(near[:-1])
+    upward(near[:-1], polls=(2,))
+    feed(near[-1:])
+    upward(near[-1:], skip=len(near) - 1)
     downward(near, polls=(1, 2))
     give_near()
     poll(len(agenda) - 1)

time: 71.7 us -> 72 us (level)
  no operation moved by 1% of the time
where the time goes in v7:
time: 72 us; the launch traced here: 71.9 us
  Pallas kernels  71 us (99%)
  between operations  0.81 us (1%)
    pallas_call x1, Pallas kernels, whole_block(): pl.pallas_call(functools.partial(block_kernel, cap), in_specs=[pl.BlockSp...  70.2 us

profile of v7, /device:TPU:0, one launch (start us, length us, event | category | flops | bytes accessed | tf_op | source)
XLA Modules:
  0.0 71.9 jit_solution(17801116322149011340)
XLA Ops:
  0.6 70.2 %shard_map.176 = (bf16[256,512]{1,0:T(8,128)(2,1)S(1)}, bf16[256,512]{1,0:T(8,128)(2,1)S(1)}) custom-call(bf16[256,512]{1,0:T(8,128)(2,1)} %mix_hbm.1, bf16[16,128]{1,0:T(8,128)(2,1)} %bitcast.6, bf16[2048,512]{1,0:T(8,128)(2,1)} %wq_hbm.1, bf16[2048,512]{1,0:T(8,128)(2,1)} %wf_hbm.1, bf16[2048,512]{1,0:T(8,128)(2,1)} %wi_hbm.1, bf16[2048,512]{1,0:T(8,128)(2,1)} %wo_hbm.1, ...), custom_call_target="tpu_custom_call" | custom-call | tf_op jit(solution)/shard_map/pallas_call | solution.py:756
  70.9 0.8 %shard_map.177 = (bf16[256,512]{1,0:T(8,128)(2,1)}, bf16[256,512]{1,0:T(8,128)(2,1)}) custom-call(bf16[256,512]{1,0:T(8,128)(2,1)S(1)} %get-tuple-element.4.a_ref, bf16[256,512]{1,0:T(8,128)(2,1)S(1)} %get-tuple-element.5.b_ref), custom_call_target="tpu_custom_call" | custom-call | tf_op jit(solution)/shard_map/pallas_call | solution.py:765
